TPU v7x, 32 devices: a whole 2x2x4 slice. The times are simulated.
32 devices in a mesh: ep: 8 (over z, x), tp: 4 (over y, core).
Axes of the slice: x: 2, y: 2, z: 4, core: 2. Of those that a mesh axis runs over, the one named last changes fastest.
Arguments:
- mixer_input: bfloat16 [4096, 2048], P('ep', 'tp'), may hold values from -6 to 6
- mixer_gain: float32 [2048], replicated, may hold values from 0.1 to 1.9
- w_query: bfloat16 [2048, 1024], P(None, 'tp'), may hold values from -0.125 to 0.125
- w_key: bfloat16 [2048, 128], replicated, may hold values from -0.125 to 0.125
- w_value: bfloat16 [2048, 128], replicated, may hold values from -0.125 to 0.125
- query_gain: float32 [64], replicated, may hold values from 0.5 to 10
- key_gain: float32 [64], replicated, may hold values from 0.5 to 10
- sink_logit: float32 [16], P('tp'), may hold values from 1 to 5
- w_output: bfloat16 [1024, 2048], P('tp'), may hold values from -0.1875 to 0.1875
- expert_input: bfloat16 [1024, 2048], P('ep'), may hold values from -6 to 6
- expert_gain: float32 [2048], replicated, may hold values from 0.1 to 1.9
- route_ids: int32 [1024, 4], P('ep'), may hold values from 0 to 7, all different within a row; in each aligned block of 128 rows (0 to 127, 128 to 255, ...) at most 128 rows name the same one
- route_weight: float32 [1024, 4], P('ep'), may hold values from 0.2 to 1.2
- expert_gate: bfloat16 [8, 2048, 2048], P('ep', None, 'tp'), may hold values from -0.125 to 0.125
- expert_up: bfloat16 [8, 2048, 2048], P('ep', None, 'tp'), may hold values from -0.125 to 0.125
- expert_down: bfloat16 [8, 2048, 2048], P('ep', None, 'tp'), may hold values from -0.125 to 0.125
- shared_gate: bfloat16 [2048, 1024], P(None, 'tp'), may hold values from -0.125 to 0.125
- shared_up: bfloat16 [2048, 1024], P(None, 'tp'), may hold values from -0.125 to 0.125
- shared_down: bfloat16 [1024, 2048], P(None, 'tp'), may hold values from -0.1875 to 0.1875
Outputs:
- mixer_output: bfloat16 [4096, 2048], P('ep', 'tp')
- expert_output: bfloat16 [1024, 2048], P('ep', 'tp')
Inputs may be any that keep to these rules, and one draw needn't show every extreme that they name: `route_ids`: each row names 4 different experts. In the rows of one index of ep (aligned blocks of 128 rows) no expert is named by more than 128 rows, a bound that some block reaches.
All inputs are finite; a program needn't handle non-finite values.
Results may differ from a plain program's by a relative error of at most 0.018.
The roundings to bfloat16 on the way count: a program that leaves them out, or rounds other values in their place, can miss the bound.
Values may be sent and summed in bfloat16 or wider, within the bound.
A program may use at most 64 MiB of HBM per device.

v0:
```python
import functools

import jax
import jax.numpy as jnp
from jax import lax
from jax.experimental import pallas as pl
from jax.experimental.pallas import tpu as pltpu
from jax.sharding import PartitionSpec as P

D = 2048
HEAD = 64
KV_HEADS = 2
WINDOW = 128
TOPK = 4


EPSILON = 1e-06


def from_behind(value, axis, steps):
    count = lax.axis_size(axis)
    first, last = (max(0, -steps), min(count, count - steps))
    return lax.ppermute(value, axis, [(source, source + steps) for source in range(first, last)])


def head_norm(matrix, gain_vector):
    return (
        matrix
        * lax.rsqrt(jnp.mean(matrix * matrix, axis=-1, keepdims=True) + EPSILON)
        * gain_vector
    )


def band_attend(queries, keys_own, values_own, keys_prev, values_prev, sink_logit, first_row):
    row_count = queries.shape[0]
    head_count = queries.shape[1]
    blocks = row_count // WINDOW
    keys_all = jnp.concatenate([keys_prev, keys_own], axis=0)
    values_all = jnp.concatenate([values_prev, values_own], axis=0)
    key_band = jnp.concatenate(
        [
            keys_all[:row_count].reshape(blocks, WINDOW, HEAD),
            keys_own.reshape(blocks, WINDOW, HEAD),
        ],
        axis=1,
    )
    value_band = jnp.concatenate(
        [
            values_all[:row_count].reshape(blocks, WINDOW, HEAD),
            values_own.reshape(blocks, WINDOW, HEAD),
        ],
        axis=1,
    )
    query_blocks = queries.reshape(blocks, WINDOW, head_count, HEAD)
    scores = jnp.einsum(
        "nqhd,nkd->nhqk", query_blocks, key_band, preferred_element_type=jnp.float32
    ) * HEAD ** (-0.5)
    query_idx = jnp.arange(WINDOW, dtype=jnp.int32)[:, None]
    key_idx = jnp.arange(2 * WINDOW, dtype=jnp.int32)[None, :]
    relative = query_idx + WINDOW - key_idx
    block_idx = jnp.arange(blocks, dtype=jnp.int32)[:, None, None]
    key_pos = first_row + block_idx * WINDOW - WINDOW + key_idx[None]
    allowed = ((relative >= 0) & (relative < WINDOW))[None] & (key_pos >= 0)
    allowed = allowed[:, None]
    masked = jnp.where(allowed, scores, -jnp.inf)
    sink_column = sink_logit.reshape(1, head_count, 1, 1)
    peak_score = jnp.maximum(jnp.max(masked, axis=-1, keepdims=True), sink_column)
    exponent = jnp.exp(masked - peak_score)
    denominator = jnp.sum(exponent, axis=-1, keepdims=True) + jnp.exp(sink_column - peak_score)
    probability = (exponent / denominator).astype(jnp.bfloat16)
    mixed_rows = jnp.einsum(
        "nhqk,nkd->nqhd", probability, value_band, preferred_element_type=jnp.float32
    )
    return mixed_rows.reshape(row_count, head_count * HEAD).astype(jnp.bfloat16)


def shards_routed(
    mixer_input,
    mixer_gain,
    w_query,
    w_key,
    w_value,
    query_gain,
    key_gain,
    sink_logit,
    w_output,
    expert_input,
    expert_gain,
    route_ids,
    route_weight,
    expert_gate,
    expert_up,
    expert_down,
    shared_gate,
    shared_up,
    shared_down,
):
    tp_count = lax.axis_size("tp")
    ep_count = lax.axis_size("ep")
    rows_local = mixer_input.shape[0]
    heads_local = w_query.shape[1] // HEAD
    kv_index = lax.axis_index("tp") // (tp_count // KV_HEADS)
    key_cols = lax.dynamic_slice_in_dim(w_key, kv_index * HEAD, HEAD, 1)
    value_cols = lax.dynamic_slice_in_dim(w_value, kv_index * HEAD, HEAD, 1)
    portion_float = lax.all_gather(mixer_input, "tp", axis=1, tiled=True).astype(jnp.float32)
    scaled = (portion_float * mixer_gain).astype(jnp.bfloat16)
    query_raw = jnp.dot(scaled, w_query, preferred_element_type=jnp.float32)
    key_raw = jnp.dot(scaled, key_cols, preferred_element_type=jnp.float32)
    value_raw = jnp.dot(scaled, value_cols, preferred_element_type=jnp.float32)
    squares = jnp.sum(portion_float * portion_float, axis=1)
    inv_rms = lax.rsqrt(squares / D + EPSILON)[:, None]
    queries = head_norm(query_raw.reshape(rows_local, heads_local, HEAD), query_gain).astype(
        jnp.bfloat16
    )
    keys_own = head_norm(key_raw, key_gain).astype(jnp.bfloat16)
    values_own = (value_raw * inv_rms).astype(jnp.bfloat16)
    keys_prev, values_prev = from_behind(
        (keys_own[rows_local - WINDOW :], values_own[rows_local - WINDOW :]), "ep", 1
    )
    first_row = lax.axis_index("ep") * rows_local
    attended = band_attend(
        queries, keys_own, values_own, keys_prev, values_prev, sink_logit, first_row
    )
    head_partial = jnp.dot(attended, w_output, preferred_element_type=jnp.float32)
    mixer_output = lax.psum_scatter(
        head_partial.astype(jnp.bfloat16), "tp", scatter_dimension=1, tiled=True
    )
    tokens_local = expert_input.shape[0]
    expert_float = expert_input.astype(jnp.float32)
    normed = (
        expert_float
        * lax.rsqrt(jnp.mean(expert_float * expert_float, axis=-1, keepdims=True) + EPSILON)
        * expert_gain
    ).astype(jnp.bfloat16)
    capacity = 2 * tokens_local * TOPK // ep_count
    flat_ids = route_ids.reshape(-1)
    onehot = (flat_ids[:, None] == jnp.arange(ep_count, dtype=jnp.int32)[None, :]).astype(jnp.int32)
    earlier = jnp.cumsum(onehot, axis=0) - onehot
    slot_index = jnp.sum(earlier * onehot, axis=-1)
    slot_column = flat_ids * capacity + slot_index
    token_ids = jnp.arange(tokens_local * TOPK, dtype=jnp.int32) // TOPK
    slot_table = (
        jnp.full((ep_count * capacity,), tokens_local, jnp.int32).at[slot_column].set(token_ids)
    )
    col_width = expert_down.shape[2]
    arrived_rows = ep_count * capacity
    own_columns = lax.dynamic_slice_in_dim(normed, lax.axis_index("tp") * col_width, col_width, 1)
    padded = jnp.concatenate([own_columns, jnp.zeros((1, col_width), jnp.bfloat16)], axis=0)
    outgoing = padded[slot_table].reshape(ep_count, capacity, col_width)
    arrived = lax.all_to_all(outgoing, "ep", split_axis=0, concat_axis=0, tiled=True).reshape(
        arrived_rows, col_width
    )
    portion = lax.all_gather(arrived, "tp", axis=1, tiled=True)
    gate_part = expert_gate[0]
    up_part = expert_up[0]
    gate_pre = jnp.dot(portion, gate_part, preferred_element_type=jnp.float32)
    up_pre = jnp.dot(portion, up_part, preferred_element_type=jnp.float32)
    routed_hidden = (jax.nn.silu(gate_pre) * up_pre).astype(jnp.bfloat16)
    shared_hidden = (
        jax.nn.silu(jnp.dot(normed, shared_gate, preferred_element_type=jnp.float32))
        * jnp.dot(normed, shared_up, preferred_element_type=jnp.float32)
    ).astype(jnp.bfloat16)
    routed_part = expert_down[0]
    routed_sum = jnp.dot(
        lax.all_gather(routed_hidden, "tp", axis=1, tiled=True),
        routed_part,
        preferred_element_type=jnp.float32,
    )
    shared_sum = jnp.dot(
        lax.all_gather(shared_hidden, "tp", axis=1, tiled=True),
        shared_down,
        preferred_element_type=jnp.float32,
    )
    expert_rows = routed_sum.astype(jnp.bfloat16).reshape(ep_count, capacity, col_width)
    returned = lax.all_to_all(expert_rows, "ep", split_axis=0, concat_axis=0, tiled=True).reshape(
        arrived_rows, col_width
    )
    picked = returned[slot_column].reshape(tokens_local, TOPK, col_width).astype(jnp.float32)
    expert_output = (shared_sum + jnp.sum(picked * route_weight[:, :, None], axis=1)).astype(
        jnp.bfloat16
    )
    return (mixer_output, expert_output)


CHUNKS = 2
COLUMNS_X = 2


def place_of(slot, ring):
    half = ring // 2
    return 0 if slot == 0 else 2 * slot - 1 if slot <= half else 2 * (ring - slot)


def ring_position(index, ring):
    row, side = index // COLUMNS_X, index % COLUMNS_X
    return row + side * (ring - 1 - 2 * row)


def ring_index(position, ring):
    side = position // (ring // COLUMNS_X)
    return 2 * position + side * (2 * ring - 1 - 4 * position)


def remote(source, target, send, receive, device):
    return pltpu.make_async_remote_copy(
        src_ref=source,
        dst_ref=target,
        send_sem=send,
        recv_sem=receive,
        device_id=device,
        device_id_type=pl.DeviceIdType.MESH,
    )


def greet(devices):
    barrier = pltpu.get_barrier_semaphore()
    for device in devices:
        pl.semaphore_signal(barrier, inc=1, device_id=device, device_id_type=pl.DeviceIdType.MESH)
    pl.semaphore_wait(barrier, len(devices))


def limit(direction, chunk, ring):
    return ring // 2 if direction == chunk else ring // 2 - 1


def slot_at(direction, distance, ring):
    return distance if direction == 0 else ring - distance


def layer_kernel(
    ring,
    rows_ref,
    gain_ref,
    dense_ref,
    mixer_ref,
    mixer_gain_ref,
    query_gain_ref,
    key_gain_ref,
    sink_ref,
    gate_hbm,
    up_hbm,
    shared_gate_hbm,
    shared_up_hbm,
    query_hbm,
    key_hbm,
    value_hbm,
    w_out_hbm,
    down_hbm,
    shared_down_hbm,
    mixer_result,
    expert_out,
    mixer_out,
    hidden_out,
    shared_out,
    dense_out,
    tok,
    gate_v,
    up_v,
    shared_gate_v,
    shared_up_v,
    query_v,
    key_v,
    value_v,
    w_out_ref,
    down_v,
    shared_down_v,
    heads_ref,
    band_ref,
    attended_ref,
    mix_buf,
    mix_got,
    mix_sum,
    mix_far,
    going,
    coming,
    own_acc,
    load_sem,
    keep_sem,
    ring_send,
    ring_recv,
    sib_send,
    sib_recv,
    mix_send,
    mix_recv,
    hid_send,
    hid_recv,
    sh_send,
    sh_recv,
    dense_send,
    dense_recv,
    halo_send,
    halo_recv,
    out_send,
    out_recv,
    back_send,
    back_recv,
):
    index, part = lax.axis_index("ep"), lax.axis_index("tp")
    far, core = part // 2, part % 2
    position = ring_position(index, ring)
    peers = [(ring_index((position + k) % ring, ring), part) for k in range(1, ring)]
    ahead, behind = peers[0], peers[-1]
    sibling = (index, 2 * far + 1 - core)
    across_part = 2 * (1 - far) + core
    across = (index, across_part)
    block, width = rows_ref.shape
    piece = block // CHUNKS
    half_width = width // 2
    hidden_width = gate_v.shape[1]

    loads = [
        pltpu.make_async_copy(source, target, load_sem.at[i])
        for i, (source, target) in enumerate(
            (
                (shared_gate_hbm, shared_gate_v),
                (shared_up_hbm, shared_up_v),
                (gate_hbm, gate_v),
                (up_hbm, up_v),
                (query_hbm, query_v),
                (key_hbm, key_v),
                (value_hbm, value_v),
                (w_out_hbm, w_out_ref),
                (down_hbm, down_v),
                (shared_down_hbm, shared_down_v),
            )
        )
    ]
    for load in loads:
        load.start()
    value = rows_ref[...].astype(jnp.float32)
    normed = (
        value
        * lax.rsqrt(jnp.mean(value * value, axis=-1, keepdims=True) + EPSILON)
        * gain_ref[...]
    ).astype(jnp.bfloat16)
    tok[0, pl.ds(0, block), :] = normed[:, :half_width]
    tok[1, pl.ds(0, block), :] = normed[:, half_width:]

    greet(peers + [sibling, across])

    def chunk_ref(half, slot, chunk):
        start = place_of(slot, ring) * block + chunk * piece
        return tok.at[half, pl.ds(start, piece), :]

    pending = []

    def start(copy):
        copy.start()
        pending.append(copy)

    def hop(direction, distance, chunk):
        start(
            remote(
                chunk_ref(core, slot_at(direction, distance - 1, ring) % ring, chunk),
                chunk_ref(core, slot_at(direction, distance, ring), chunk),
                ring_send.at[direction, distance, chunk],
                ring_recv.at[direction, distance, chunk],
                ahead if direction == 0 else behind,
            )
        )

    for chunk in range(CHUNKS):
        for direction in range(2):
            hop(direction, 1, chunk)
    mixer_pieces = mix_send.shape[1]
    mixer_rows = mixer_ref.shape[0] // mixer_pieces
    mixer_cols = mixer_ref.shape[1]

    def mixer_slice(owner, i):
        return mixer_out.at[
            pl.ds(i * mixer_rows, mixer_rows),
            pl.ds(pl.multiple_of(owner * mixer_cols, mixer_cols), mixer_cols),
        ]

    for i in range(mixer_pieces):
        own = mixer_ref.at[pl.ds(i * mixer_rows, mixer_rows), :]
        start(remote(own, mixer_slice(part, i), mix_send.at[0, i], mix_recv.at[0, i], across))
    for i in range(mixer_pieces):
        own = mixer_ref.at[pl.ds(i * mixer_rows, mixer_rows), :]
        start(remote(own, mixer_slice(part, i), mix_send.at[1, i], mix_recv.at[1, i], sibling))
    keep = pltpu.make_async_copy(
        mixer_ref,
        mixer_out.at[:, pl.ds(pl.multiple_of(part * mixer_cols, mixer_cols), mixer_cols)],
        keep_sem.at[0],
    )
    keep.start()
    for k in range(1, ring):
        start(
            remote(
                dense_ref, dense_out.at[k], dense_send.at[k], dense_recv.at[k], peers[k - 1]
            )
        )
    dense_out[0] = dense_ref[...]

    loads[0].wait()
    loads[1].wait()

    def product(first, count, weights, columns):
        low = tok[0, pl.ds(first, count), :]
        high = tok[1, pl.ds(first, count), :]
        return jnp.dot(
            low, weights[pl.ds(0, half_width), columns], preferred_element_type=jnp.float32
        ) + jnp.dot(
            high,
            weights[pl.ds(half_width, half_width), columns],
            preferred_element_type=jnp.float32,
        )

    everything = pl.ds(0, shared_gate_v.shape[1])
    shared_out[part] = (
        jax.nn.silu(product(0, block, shared_gate_v, everything))
        * product(0, block, shared_up_v, everything)
    ).astype(jnp.bfloat16)
    start(remote(shared_out.at[part], shared_out.at[part], sh_send.at[0], sh_recv.at[0], across))
    start(remote(shared_out.at[part], shared_out.at[part], sh_send.at[1], sh_recv.at[1], sibling))
    loads[2].wait()
    loads[3].wait()

    def hidden_ref(owner, slot):
        return hidden_out.at[owner, pl.ds(place_of(slot, ring) * block, block), :]

    tile = 256

    def compute(slots):
        first = min(place_of(slot, ring) for slot in slots) * block
        count = len(slots) * block

        def one(j, carry):
            columns = pl.ds(pl.multiple_of(j * tile, tile), tile)
            hidden_out[part, pl.ds(first, count), columns] = (
                jax.nn.silu(product(first, count, gate_v, columns))
                * product(first, count, up_v, columns)
            ).astype(jnp.bfloat16)
            return carry

        lax.fori_loop(0, hidden_width // tile, one, 0)
        for slot in slots:
            own = hidden_ref(part, slot)
            start(remote(own, own, hid_send.at[0, slot], hid_recv.at[0, slot], across))
            start(remote(own, own, hid_send.at[1, slot], hid_recv.at[1, slot], sibling))

    def arrive(distance):
        for chunk in range(CHUNKS):
            for direction in range(2):
                if distance > limit(direction, chunk, ring):
                    continue
                slot = slot_at(direction, distance, ring)
                here = chunk_ref(core, slot, chunk)
                remote(
                    here,
                    here,
                    ring_send.at[direction, distance, chunk],
                    ring_recv.at[direction, distance, chunk],
                    sibling,
                ).wait_recv()
                if distance < limit(direction, chunk, ring):
                    hop(direction, distance + 1, chunk)
                start(
                    remote(
                        here,
                        here,
                        sib_send.at[direction, distance, chunk],
                        sib_recv.at[direction, distance, chunk],
                        sibling,
                    )
                )

    def swapped(distance):
        for chunk in range(CHUNKS):
            for direction in range(2):
                if distance > limit(direction, chunk, ring):
                    continue
                there = chunk_ref(1 - core, slot_at(direction, distance, ring), chunk)
                remote(
                    there,
                    there,
                    sib_send.at[direction, distance, chunk],
                    sib_recv.at[direction, distance, chunk],
                    sibling,
                ).wait_recv()

    def forward_mixer():
        for i in range(mixer_pieces):
            here = mixer_slice(across_part, i)
            remote(here, here, mix_send.at[0, i], mix_recv.at[0, i], sibling).wait_recv()
            start(remote(here, here, mix_send.at[2, i], mix_recv.at[2, i], sibling))

    def forward_hidden(slots):
        for slot in slots:
            here = hidden_ref(across_part, slot)
            remote(here, here, hid_send.at[0, slot], hid_recv.at[0, slot], sibling).wait_recv()
            start(remote(here, here, hid_send.at[2, slot], hid_recv.at[2, slot], sibling))

    steps = ring // 2
    compute([0])
    arrive(1)
    for distance in range(1, steps + 1):
        swapped(distance)
        if distance < steps:
            compute([distance, ring - distance])
            arrive(distance + 1)
            if distance == steps - 2:
                forward_mixer()
        else:
            compute([distance])
    order = [0]
    for distance in range(1, steps):
        order += [distance, ring - distance]
    order += [steps]
    forward_hidden(order[:3])

    sib_part = 2 * far + 1 - core
    corner = 2 * (1 - far) + 1 - core
    for path, owner in ((1, sib_part), (2, corner)):
        for i in range(mixer_pieces):
            here = mixer_slice(owner, i)
            remote(here, here, mix_send.at[path, i], mix_recv.at[path, i], sibling).wait_recv()
    keep.wait()
    for load in loads[4:8]:
        load.wait()
    rows_local = mixer_ref.shape[0]
    query_sum = key_sum = value_sum = squares = 0.0
    for owner in range(mixer_out.shape[1] // mixer_cols):
        columns = pl.ds(owner * mixer_cols, mixer_cols)
        value = mixer_out[:, columns].astype(jnp.float32)
        squares = squares + jnp.sum(value * value, axis=1, keepdims=True)
        scaled = (value * mixer_gain_ref[:, columns]).astype(jnp.bfloat16)
        query_sum = query_sum + jnp.dot(
            scaled, query_v[columns, :], preferred_element_type=jnp.float32
        )
        key_sum = key_sum + jnp.dot(
            scaled, key_v[columns, :], preferred_element_type=jnp.float32
        )
        value_sum = value_sum + jnp.dot(
            scaled, value_v[columns, :], preferred_element_type=jnp.float32
        )
    second = part // (lax.axis_size("tp") // KV_HEADS)
    key_raw = jnp.where(second == 0, key_sum[:, :HEAD], key_sum[:, HEAD:])
    value_raw = jnp.where(second == 0, value_sum[:, :HEAD], value_sum[:, HEAD:])
    band_ref[pl.ds(WINDOW, rows_local), :] = jnp.concatenate(
        [
            head_norm(key_raw, key_gain_ref[...]),
            value_raw * lax.rsqrt(squares / D + EPSILON),
        ],
        axis=1,
    ).astype(jnp.bfloat16)
    heads_local = heads_ref.shape[0]
    for head in range(heads_local):
        one_head = query_sum[:, head * HEAD : (head + 1) * HEAD]
        heads_ref[head] = head_norm(one_head, query_gain_ref[...]).astype(jnp.bfloat16)
    start(
        remote(
            band_ref.at[pl.ds(rows_local, WINDOW), :],
            band_ref.at[pl.ds(0, WINDOW), :],
            halo_send.at[0],
            halo_recv.at[0],
            ((index + 1) % ring, part),
        )
    )
    forward_hidden(order[3:5])
    halo = band_ref.at[pl.ds(0, WINDOW), :]
    remote(halo, halo, halo_send.at[0], halo_recv.at[0], sibling).wait_recv()
    query_rows = heads_local * WINDOW
    row_idx = lax.broadcasted_iota(jnp.int32, (query_rows, 2 * WINDOW), 0) % WINDOW
    key_idx = lax.broadcasted_iota(jnp.int32, (query_rows, 2 * WINDOW), 1)
    relative = row_idx + WINDOW - key_idx
    in_window = (relative >= 0) & (relative < WINDOW)

    def attend(i, carry):
        first = pl.multiple_of(i * WINDOW, WINDOW)
        block_queries = heads_ref[:, pl.ds(first, WINDOW), :].reshape(query_rows, HEAD)
        band = band_ref[pl.ds(first, 2 * WINDOW), :]
        scores = lax.dot_general(
            block_queries,
            band[:, :HEAD],
            (((1,), (1,)), ((), ())),
            preferred_element_type=jnp.float32,
        ) * HEAD ** (-0.5)
        key_pos = index * rows_local + first - WINDOW + key_idx
        masked = jnp.where(in_window & (key_pos >= 0), scores, -jnp.inf)
        sink = sink_ref[...]
        peak = jnp.maximum(jnp.max(masked, axis=-1, keepdims=True), sink)
        exponent = jnp.exp(masked - peak)
        denominator = jnp.sum(exponent, axis=-1, keepdims=True) + jnp.exp(sink - peak)
        probability = (exponent / denominator).astype(jnp.bfloat16)
        mixed = jnp.dot(probability, band[:, HEAD:], preferred_element_type=jnp.float32)
        attended_ref[pl.ds(first, WINDOW), :] = jnp.concatenate(
            [mixed[head * WINDOW : (head + 1) * WINDOW] for head in range(heads_local)], axis=1
        ).astype(jnp.bfloat16)
        return carry

    lax.fori_loop(0, rows_local // WINDOW, attend, 0)

    parts, block, shared_width = shared_out.shape
    width = down_v.shape[1]
    inner = hidden_out.shape[2]
    def head_block(owner):
        columns = pl.ds(pl.multiple_of(owner * width, width), width)
        return jnp.dot(
            attended_ref[...], w_out_ref[:, columns], preferred_element_type=jnp.float32
        ).astype(jnp.bfloat16)

    mix_buf[0] = head_block(2 * (1 - far) + 1 - core)
    mix_buf[1] = head_block(2 * far + 1 - core)
    for i in range(2):
        start(remote(mix_buf.at[i], mix_got.at[i], out_send.at[i], out_recv.at[i], sibling))
    mix_buf[2] = head_block(across_part)
    mix_buf[3] = head_block(part)

    forward_hidden(order[5:])
    here = shared_out.at[across_part]
    remote(here, here, sh_send.at[0], sh_recv.at[0], sibling).wait_recv()
    start(remote(here, here, sh_send.at[2], sh_recv.at[2], sibling))
    for peer in range(1, ring):
        here = dense_out.at[peer]
        remote(here, here, dense_send.at[peer], dense_recv.at[peer], sibling).wait_recv()
    for path, owner in ((1, sib_part), (2, corner)):
        here = shared_out.at[owner]
        remote(here, here, sh_send.at[path], sh_recv.at[path], sibling).wait_recv()
        for slot in order:
            here = hidden_ref(owner, slot)
            remote(
                here, here, hid_send.at[path, slot], hid_recv.at[path, slot], sibling
            ).wait_recv()
    loads[8].wait()
    diagonal = lax.broadcasted_iota(jnp.int32, (block, block), 0) == lax.broadcasted_iota(
        jnp.int32, (block, block), 1
    )

    def weight_column(slot):
        row = dense_out[slot, pl.ds(index, 1), :]
        return jnp.sum(jnp.where(diagonal, row, 0.0), axis=1, keepdims=True)


    def weighted(slots):
        first = min(place_of(slot, ring) for slot in slots) * block
        count = len(slots) * block
        total = jnp.dot(
            hidden_out[0, pl.ds(first, count), :],
            down_v[pl.ds(0, inner), :],
            preferred_element_type=jnp.float32,
        )
        for owner in range(1, parts):
            total = total + jnp.dot(
                hidden_out[owner, pl.ds(first, count), :],
                down_v[pl.ds(owner * inner, inner), :],
                preferred_element_type=jnp.float32,
            )
        rounded = total.astype(jnp.bfloat16).astype(jnp.float32)
        ordered = sorted(slots, key=lambda slot: place_of(slot, ring))
        return rounded * jnp.concatenate([weight_column(slot) for slot in ordered], axis=0)

    def received(direction, distance, chunk):
        return coming.at[direction, distance, pl.ds(chunk * piece, piece), :]

    def wait_for(direction, distance, chunk):
        here = received(direction, distance, chunk)
        remote(
            here,
            here,
            back_send.at[direction, distance, chunk],
            back_recv.at[direction, distance, chunk],
            ahead,
        ).wait_recv()
        return here[...].astype(jnp.float32)

    def push(distance, values):
        for chunk in range(CHUNKS):
            for direction in range(2):
                longest = limit(direction, chunk, ring)
                if distance > longest:
                    continue
                value = values[direction][chunk * piece : (chunk + 1) * piece]
                if distance < longest:
                    value = value + wait_for(direction, distance + 1, chunk)
                rows = pl.ds(chunk * piece, piece)
                going[direction, distance, rows, :] = value.astype(jnp.bfloat16)
                start(
                    remote(
                        going.at[direction, distance, rows, :],
                        received(direction, distance, chunk),
                        back_send.at[direction, distance, chunk],
                        back_recv.at[direction, distance, chunk],
                        ahead if direction == 0 else behind,
                    )
                )

    farthest = weighted([steps])
    push(steps, (farthest, farthest))
    for i in range(2):
        remote(
            mix_got.at[i], mix_got.at[i], out_send.at[i], out_recv.at[i], sibling
        ).wait_recv()
    mix_sum[...] = (
        mix_buf[2].astype(jnp.float32) + mix_got[0].astype(jnp.float32)
    ).astype(jnp.bfloat16)
    start(remote(mix_sum, mix_far, out_send.at[2], out_recv.at[2], across))
    for distance in range(steps - 1, 0, -1):
        both = weighted([distance, ring - distance])
        push(distance, (both[block:], both[:block]))
    own = weighted([0])
    loads[9].wait()
    for owner in range(parts):
        own = own + jnp.dot(
            shared_out[owner],
            shared_down_v[pl.ds(owner * shared_width, shared_width), :],
            preferred_element_type=jnp.float32,
        )
    own_acc[...] = own
    for chunk in range(CHUNKS):
        rows = pl.ds(chunk * piece, piece)
        expert_out[rows, :] = (
            own_acc[rows, :] + wait_for(0, 1, chunk) + wait_for(1, 1, chunk)
        ).astype(jnp.bfloat16)
    remote(mix_far, mix_far, out_send.at[2], out_recv.at[2], sibling).wait_recv()
    mixer_result[...] = (
        mix_buf[3].astype(jnp.float32)
        + mix_got[1].astype(jnp.float32)
        + mix_far[...].astype(jnp.float32)
    ).astype(jnp.bfloat16)
    for copy in pending:
        copy.wait_send()


def shards(
    mixer_input,
    mixer_gain,
    w_query,
    w_key,
    w_value,
    query_gain,
    key_gain,
    sink_logit,
    w_output,
    expert_input,
    expert_gain,
    route_ids,
    route_weight,
    expert_gate,
    expert_up,
    expert_down,
    shared_gate,
    shared_up,
    shared_down,
):
    ring = lax.axis_size("ep")
    parts = lax.axis_size("tp")
    rows_local, mixer_cols = mixer_input.shape
    tokens_local, width = expert_input.shape
    hidden_width = expert_gate.shape[2]
    shared_width = shared_gate.shape[1]
    out_width = expert_down.shape[2]
    half = ring // 2
    vmem = pl.BlockSpec(memory_space=pltpu.VMEM)
    hbm = pl.BlockSpec(memory_space=pl.ANY)
    bf16, f32 = jnp.bfloat16, jnp.float32
    dma = pltpu.SemaphoreType.DMA
    chosen = route_ids[:, :, None] == jnp.arange(ring, dtype=jnp.int32)
    dense = jnp.sum(jnp.where(chosen, route_weight[:, :, None], 0.0), axis=1).T
    mixer_pieces = 4
    heads_local = w_query.shape[1] // HEAD
    vm = pltpu.VMEM
    return pl.pallas_call(
        functools.partial(layer_kernel, ring),
        out_shape=(
            jax.ShapeDtypeStruct((rows_local, out_width), bf16),
            jax.ShapeDtypeStruct((tokens_local, out_width), bf16),
        ),
        in_specs=[vmem] * 8 + [hbm] * 10,
        out_specs=(vmem,) * 2,
        scratch_shapes=[
            vm((rows_local, parts * mixer_cols), bf16),
            vm((parts, ring * tokens_local, hidden_width), bf16),
            vm((parts, tokens_local, shared_width), bf16),
            vm((ring, ring, tokens_local), f32),
            vm((2, ring * tokens_local, width // 2), bf16),
            vm((width, hidden_width), bf16),
            vm((width, hidden_width), bf16),
            vm((width, shared_width), bf16),
            vm((width, shared_width), bf16),
            vm(w_query.shape, bf16),
            vm(w_key.shape, bf16),
            vm(w_value.shape, bf16),
            vm(w_output.shape, bf16),
            vm(expert_down.shape[1:], bf16),
            vm(shared_down.shape, bf16),
            vm((heads_local, rows_local, HEAD), bf16),
            vm((WINDOW + rows_local, 2 * HEAD), bf16),
            vm((rows_local, heads_local * HEAD), bf16),
            vm((4, rows_local, out_width), bf16),
            vm((2, rows_local, out_width), bf16),
            vm((rows_local, out_width), bf16),
            vm((rows_local, out_width), bf16),
            vm((2, half + 1, tokens_local, out_width), bf16),
            vm((2, half + 1, tokens_local, out_width), bf16),
            vm((tokens_local, out_width), f32),
            dma((10,)),
            dma((1,)),
            dma((2, half + 1, CHUNKS)),
            dma((2, half + 1, CHUNKS)),
            dma((2, half + 1, CHUNKS)),
            dma((2, half + 1, CHUNKS)),
            dma((3, mixer_pieces)),
            dma((3, mixer_pieces)),
            dma((3, ring)),
            dma((3, ring)),
            dma((3,)),
            dma((3,)),
            dma((ring,)),
            dma((ring,)),
            dma((1,)),
            dma((1,)),
            dma((3,)),
            dma((3,)),
            dma((2, half + 1, CHUNKS)),
            dma((2, half + 1, CHUNKS)),
        ],
        compiler_params=pltpu.CompilerParams(
            collective_id=0, has_side_effects=True, vmem_limit_bytes=62 * 1024 * 1024
        ),
        name="layer",
    )(
        expert_input,
        expert_gain[None, :],
        dense,
        mixer_input,
        mixer_gain[None, :],
        query_gain[None, :],
        key_gain[None, :],
        jnp.repeat(sink_logit, WINDOW)[:, None],
        expert_gate[0],
        expert_up[0],
        shared_gate,
        shared_up,
        w_query,
        w_key,
        w_value,
        w_output,
        expert_down[0],
        shared_down,
    )


def plan(*arrays):
    route_ids = arrays[11]
    capacity = 2 * route_ids.size // lax.axis_size("ep")
    whole_blocks = capacity >= route_ids.shape[0]
    if whole_blocks and lax.axis_size("tp") == 4:
        return shards(*arrays)
    return shards_routed(*arrays)


def solution(mesh):
    in_specs = (
        P("ep", "tp"),
        P(),
        P(None, "tp"),
        P(),
        P(),
        P(),
        P(),
        P("tp"),
        P("tp", None),
        P("ep", None),
        P(),
        P("ep", None),
        P("ep", None),
        P("ep", None, "tp"),
        P("ep", None, "tp"),
        P("ep", None, "tp"),
        P(None, "tp"),
        P(None, "tp"),
        P(None, "tp"),
    )
    out_specs = (P("ep", "tp"), P("ep", "tp"))
    return jax.shard_map(plan, mesh=mesh, in_specs=in_specs, out_specs=out_specs, check_vma=False)
```

profile of v0, /device:TPU:0, one launch (start us, length us, event | category | flops | bytes accessed | tf_op | source)
XLA Modules:
  0.0 76.9 jit_solution(11663928686492068875)
XLA Ops:
  0.6 0.7 broadcast_in_dim.36
  1.4 1.3 %select_reduce_fusion = f32[128,8]{0,1:T(8,128)} fusion(f32[128,4]{0,1:T(4,128)} %param.31, s32[128,4]{0,1:T(4,128)} %param.30), kind=kLoop, calls=%fused_computation | loop fusion | flops 11264 | bytes 8192 | tf_op jit(solution)/shard_map/reduce_sum | solution.py:759
  2.7 0.9 %copy.26.sink_ref = f32[512,1]{1,0:T(8,128)} copy(f32[512,1]{0,1:T(1,128)S(1)} %bitcast.13) | data formatting | bytes 4096 | tf_op jit(solution)/shard_map/broadcast_in_dim;reshape | solution.py:830
  3.5 70.0 %layer.1 = (bf16[512,512]{1,0:T(8,128)(2,1)}, bf16[128,512]{1,0:T(8,128)(2,1)}) custom-call(bf16[128,2048]{1,0:T(8,128)(2,1)} %rows_ref.1, f32[1,2048]{1,0:T(1,128)} %bitcast.14, f32[8,128]{1,0:T(8,128)} %bitcast.12, bf16[512,512]{1,0:T(8,128)(2,1)} %mixer_ref.1, f32[1,2048]{1,0:T(1,128)} %bitcast.15, f32[1,64]{1,0:T(1,128)} %bitcast.16, f32[1,64]{1,0:T(1,128)} %bitcast.17, ...), custom_call_target="tpu_custom_call" | custom-call | tf_op jit(solution)/shard_map/layer/pallas_call | solution.py:763
  73.5 1.9 %copy.29 = bf16[512,512]{1,0:T(8,128)(2,1)} copy(bf16[512,512]{1,0:T(8,128)(2,1)} %get-tuple-element.4) | data formatting | bytes 1048576
  75.4 1.6 %copy.30 = bf16[128,512]{1,0:T(8,128)(2,1)} copy(bf16[128,512]{1,0:T(8,128)(2,1)} %get-tuple-element.5) | data formatting | bytes 262144
where the time goes:
time: 77.2 us; the launch traced here: 76.9 us
  Pallas kernels  70 us (91%)
  local copies, waits for them, and re-layouts  5.02 us (7%)
  other arithmetic  1.3 us (2%)
    pallas_call x1, Pallas kernels, shards(): pl.pallas_call(functools.partial(layer_kernel, ring), out_shape=(jax.Shap...  70 us
    unnamed x2, local copies, waits for them, and re-layouts  3.44 us

commit v1 on v0

v1 whole, which is shorter than its diff:
```python
import functools

import jax
import jax.numpy as jnp
from jax import lax
from jax.experimental import pallas as pl
from jax.experimental.pallas import tpu as pltpu
from jax.sharding import PartitionSpec as P

D = 2048
HEAD = 64
KV_HEADS = 2
WINDOW = 128
TOPK = 4


EPSILON = 1e-06


def from_behind(value, axis, steps):
    count = lax.axis_size(axis)
    first, last = (max(0, -steps), min(count, count - steps))
    return lax.ppermute(value, axis, [(source, source + steps) for source in range(first, last)])


def head_norm(matrix, gain_vector):
    return (
        matrix
        * lax.rsqrt(jnp.mean(matrix * matrix, axis=-1, keepdims=True) + EPSILON)
        * gain_vector
    )


def band_attend(queries, keys_own, values_own, keys_prev, values_prev, sink_logit, first_row):
    row_count = queries.shape[0]
    head_count = queries.shape[1]
    blocks = row_count // WINDOW
    keys_all = jnp.concatenate([keys_prev, keys_own], axis=0)
    values_all = jnp.concatenate([values_prev, values_own], axis=0)
    key_band = jnp.concatenate(
        [
            keys_all[:row_count].reshape(blocks, WINDOW, HEAD),
            keys_own.reshape(blocks, WINDOW, HEAD),
        ],
        axis=1,
    )
    value_band = jnp.concatenate(
        [
            values_all[:row_count].reshape(blocks, WINDOW, HEAD),
            values_own.reshape(blocks, WINDOW, HEAD),
        ],
        axis=1,
    )
    query_blocks = queries.reshape(blocks, WINDOW, head_count, HEAD)
    scores = jnp.einsum(
        "nqhd,nkd->nhqk", query_blocks, key_band, preferred_element_type=jnp.float32
    ) * HEAD ** (-0.5)
    query_idx = jnp.arange(WINDOW, dtype=jnp.int32)[:, None]
    key_idx = jnp.arange(2 * WINDOW, dtype=jnp.int32)[None, :]
    relative = query_idx + WINDOW - key_idx
    block_idx = jnp.arange(blocks, dtype=jnp.int32)[:, None, None]
    key_pos = first_row + block_idx * WINDOW - WINDOW + key_idx[None]
    allowed = ((relative >= 0) & (relative < WINDOW))[None] & (key_pos >= 0)
    allowed = allowed[:, None]
    masked = jnp.where(allowed, scores, -jnp.inf)
    sink_column = sink_logit.reshape(1, head_count, 1, 1)
    peak_score = jnp.maximum(jnp.max(masked, axis=-1, keepdims=True), sink_column)
    exponent = jnp.exp(masked - peak_score)
    denominator = jnp.sum(exponent, axis=-1, keepdims=True) + jnp.exp(sink_column - peak_score)
    probability = (exponent / denominator).astype(jnp.bfloat16)
    mixed_rows = jnp.einsum(
        "nhqk,nkd->nqhd", probability, value_band, preferred_element_type=jnp.float32
    )
    return mixed_rows.reshape(row_count, head_count * HEAD).astype(jnp.bfloat16)


def shards_routed(
    mixer_input,
    mixer_gain,
    w_query,
    w_key,
    w_value,
    query_gain,
    key_gain,
    sink_logit,
    w_output,
    expert_input,
    expert_gain,
    route_ids,
    route_weight,
    expert_gate,
    expert_up,
    expert_down,
    shared_gate,
    shared_up,
    shared_down,
):
    tp_count = lax.axis_size("tp")
    ep_count = lax.axis_size("ep")
    rows_local = mixer_input.shape[0]
    heads_local = w_query.shape[1] // HEAD
    kv_index = lax.axis_index("tp") // (tp_count // KV_HEADS)
    key_cols = lax.dynamic_slice_in_dim(w_key, kv_index * HEAD, HEAD, 1)
    value_cols = lax.dynamic_slice_in_dim(w_value, kv_index * HEAD, HEAD, 1)
    portion_float = lax.all_gather(mixer_input, "tp", axis=1, tiled=True).astype(jnp.float32)
    scaled = (portion_float * mixer_gain).astype(jnp.bfloat16)
    query_raw = jnp.dot(scaled, w_query, preferred_element_type=jnp.float32)
    key_raw = jnp.dot(scaled, key_cols, preferred_element_type=jnp.float32)
    value_raw = jnp.dot(scaled, value_cols, preferred_element_type=jnp.float32)
    squares = jnp.sum(portion_float * portion_float, axis=1)
    inv_rms = lax.rsqrt(squares / D + EPSILON)[:, None]
    queries = head_norm(query_raw.reshape(rows_local, heads_local, HEAD), query_gain).astype(
        jnp.bfloat16
    )
    keys_own = head_norm(key_raw, key_gain).astype(jnp.bfloat16)
    values_own = (value_raw * inv_rms).astype(jnp.bfloat16)
    keys_prev, values_prev = from_behind(
        (keys_own[rows_local - WINDOW :], values_own[rows_local - WINDOW :]), "ep", 1
    )
    first_row = lax.axis_index("ep") * rows_local
    attended = band_attend(
        queries, keys_own, values_own, keys_prev, values_prev, sink_logit, first_row
    )
    head_partial = jnp.dot(attended, w_output, preferred_element_type=jnp.float32)
    mixer_output = lax.psum_scatter(
        head_partial.astype(jnp.bfloat16), "tp", scatter_dimension=1, tiled=True
    )
    tokens_local = expert_input.shape[0]
    expert_float = expert_input.astype(jnp.float32)
    normed = (
        expert_float
        * lax.rsqrt(jnp.mean(expert_float * expert_float, axis=-1, keepdims=True) + EPSILON)
        * expert_gain
    ).astype(jnp.bfloat16)
    capacity = 2 * tokens_local * TOPK // ep_count
    flat_ids = route_ids.reshape(-1)
    onehot = (flat_ids[:, None] == jnp.arange(ep_count, dtype=jnp.int32)[None, :]).astype(jnp.int32)
    earlier = jnp.cumsum(onehot, axis=0) - onehot
    slot_index = jnp.sum(earlier * onehot, axis=-1)
    slot_column = flat_ids * capacity + slot_index
    token_ids = jnp.arange(tokens_local * TOPK, dtype=jnp.int32) // TOPK
    slot_table = (
        jnp.full((ep_count * capacity,), tokens_local, jnp.int32).at[slot_column].set(token_ids)
    )
    col_width = expert_down.shape[2]
    arrived_rows = ep_count * capacity
    own_columns = lax.dynamic_slice_in_dim(normed, lax.axis_index("tp") * col_width, col_width, 1)
    padded = jnp.concatenate([own_columns, jnp.zeros((1, col_width), jnp.bfloat16)], axis=0)
    outgoing = padded[slot_table].reshape(ep_count, capacity, col_width)
    arrived = lax.all_to_all(outgoing, "ep", split_axis=0, concat_axis=0, tiled=True).reshape(
        arrived_rows, col_width
    )
    portion = lax.all_gather(arrived, "tp", axis=1, tiled=True)
    gate_part = expert_gate[0]
    up_part = expert_up[0]
    gate_pre = jnp.dot(portion, gate_part, preferred_element_type=jnp.float32)
    up_pre = jnp.dot(portion, up_part, preferred_element_type=jnp.float32)
    routed_hidden = (jax.nn.silu(gate_pre) * up_pre).astype(jnp.bfloat16)
    shared_hidden = (
        jax.nn.silu(jnp.dot(normed, shared_gate, preferred_element_type=jnp.float32))
        * jnp.dot(normed, shared_up, preferred_element_type=jnp.float32)
    ).astype(jnp.bfloat16)
    routed_part = expert_down[0]
    routed_sum = jnp.dot(
        lax.all_gather(routed_hidden, "tp", axis=1, tiled=True),
        routed_part,
        preferred_element_type=jnp.float32,
    )
    shared_sum = jnp.dot(
        lax.all_gather(shared_hidden, "tp", axis=1, tiled=True),
        shared_down,
        preferred_element_type=jnp.float32,
    )
    expert_rows = routed_sum.astype(jnp.bfloat16).reshape(ep_count, capacity, col_width)
    returned = lax.all_to_all(expert_rows, "ep", split_axis=0, concat_axis=0, tiled=True).reshape(
        arrived_rows, col_width
    )
    picked = returned[slot_column].reshape(tokens_local, TOPK, col_width).astype(jnp.float32)
    expert_output = (shared_sum + jnp.sum(picked * route_weight[:, :, None], axis=1)).astype(
        jnp.bfloat16
    )
    return (mixer_output, expert_output)


CHUNKS = 2
VMEM_LIMIT = 62 * 1024 * 1024
PARTS_BACK = 4
COLUMNS_X = 2


def place_of(slot, ring):
    half = ring // 2
    return 0 if slot == 0 else 2 * slot - 1 if slot <= half else 2 * (ring - slot)


def ring_position(index, ring):
    row, side = index // COLUMNS_X, index % COLUMNS_X
    return row + side * (ring - 1 - 2 * row)


def ring_index(position, ring):
    side = position // (ring // COLUMNS_X)
    return 2 * position + side * (2 * ring - 1 - 4 * position)


def remote(source, target, send, receive, device):
    return pltpu.make_async_remote_copy(
        src_ref=source,
        dst_ref=target,
        send_sem=send,
        recv_sem=receive,
        device_id=device,
        device_id_type=pl.DeviceIdType.MESH,
    )


def limit(direction, chunk, ring):
    return ring // 2 if direction == chunk else ring // 2 - 1


def slot_at(direction, distance, ring):
    return distance if direction == 0 else ring - distance


def layer_kernel(
    ring,
    rows_hbm,
    gain_hbm,
    ids_hbm,
    weight_hbm,
    mixer_hbm,
    mixer_gain_hbm,
    query_gain_hbm,
    key_gain_hbm,
    sink_hbm,
    gate_hbm,
    up_hbm,
    shared_gate_hbm,
    shared_up_hbm,
    query_hbm,
    key_hbm,
    value_hbm,
    w_out_hbm,
    down_hbm,
    shared_down_hbm,
    mixer_result,
    expert_result,
    rows_v,
    gain_v,
    ids_v,
    weight_v,
    mixer_gain_v,
    query_gain_v,
    key_gain_v,
    sink_v,
    mixer_all,
    hidden_all,
    shared_all,
    att_all,
    dense_all,
    tok,
    gate_v,
    up_v,
    shared_gate_v,
    shared_up_v,
    qkv_v,
    down_v,
    shared_down_v,
    out_cols,
    out_stage,
    scaled_v,
    heads_v,
    band_v,
    bias_v,
    ready,
    going,
    coming,
    mixer_v,
    expert_v,
    load_sem,
    store_sem,
    ring_send,
    ring_recv,
    sib_send,
    sib_recv,
    mix_send,
    mix_recv,
    hid_send,
    hid_recv,
    sh_send,
    sh_recv,
    att_send,
    att_recv,
    dense_send,
    dense_recv,
    halo_send,
    halo_recv,
    wcol_send,
    wcol_recv,
    wring_send,
    wring_recv,
    back_send,
    back_recv,
):
    scope = jax.named_scope
    f32, bf16 = jnp.float32, jnp.bfloat16
    index, part = lax.axis_index("ep"), lax.axis_index("tp")
    far, core = part // 2, part % 2
    position = ring_position(index, ring)
    peer_index = [ring_index((position + k) % ring, ring) for k in range(ring)]
    peers = [(peer_index[k], part) for k in range(1, ring)]
    ahead, behind = peers[0], peers[-1]
    sib_part = 2 * far + 1 - core
    across_part = 2 * (1 - far) + core
    corner_part = 2 * (1 - far) + 1 - core
    sibling, across = (index, sib_part), (index, across_part)
    block, width = rows_v.shape
    half_width = width // 2
    piece = block // CHUNKS
    steps = ring // 2
    parts, rows_local, mixer_cols = mixer_all.shape
    pieces = rows_local // WINDOW
    out_width = down_v.shape[1]
    inner = hidden_all.shape[2]
    shared_width = shared_all.shape[2]
    head_rows = out_cols.shape[1]
    share_rows = head_rows // ring
    share_piece = share_rows // CHUNKS

    barrier = pltpu.get_barrier_semaphore()
    for device in peers + [sibling, across]:
        pl.semaphore_signal(barrier, inc=1, device_id=device, device_id_type=pl.DeviceIdType.MESH)

    pending, stores = [], []

    def start(copy):
        copy.start()
        pending.append(copy)

    loads = {}

    def load(name, source, target):
        loads[name] = pltpu.make_async_copy(source, target, load_sem.at[len(loads)])
        loads[name].start()

    own_cols = pl.ds(pl.multiple_of(part * out_width, out_width), out_width)
    load("rows", rows_hbm, rows_v)
    load("gain", gain_hbm, gain_v)
    load("mixer", mixer_hbm, mixer_all.at[part])
    load("shared_gate", shared_gate_hbm, shared_gate_v)
    load("shared_up", shared_up_hbm, shared_up_v)
    load("gate", gate_hbm, gate_v)
    load("up", up_hbm, up_v)
    load("ids", ids_hbm, ids_v)
    load("weight", weight_hbm, weight_v)
    load("mixer_gain", mixer_gain_hbm, mixer_gain_v)
    load("query_gain", query_gain_hbm, query_gain_v)
    load("key_gain", key_gain_hbm, key_gain_v)
    load("sink", sink_hbm, sink_v)
    load("query", query_hbm, qkv_v.at[:, pl.ds(0, query_hbm.shape[1])])
    load("key", key_hbm, qkv_v.at[:, pl.ds(query_hbm.shape[1], key_hbm.shape[1])])
    load(
        "value",
        value_hbm,
        qkv_v.at[:, pl.ds(query_hbm.shape[1] + key_hbm.shape[1], value_hbm.shape[1])],
    )
    load("out_own", w_out_hbm.at[:, own_cols], out_cols.at[part])
    load("down", down_hbm, down_v)
    load("shared_down", shared_down_hbm, shared_down_v)

    relative = (
        lax.broadcasted_iota(jnp.int32, (WINDOW, 2 * WINDOW), 0)
        + WINDOW
        - lax.broadcasted_iota(jnp.int32, (WINDOW, 2 * WINDOW), 1)
    )
    bias_v[...] = jnp.where((relative >= 0) & (relative < WINDOW), 0.0, -jnp.inf)
    low = lax.broadcasted_iota(jnp.int32, (WINDOW, 2 * HEAD), 1) < HEAD

    with scope("norm"):
        loads["rows"].wait()
        loads["gain"].wait()
        value = rows_v[...].astype(f32)
        normed = (
            value
            * lax.rsqrt(jnp.mean(value * value, axis=-1, keepdims=True) + EPSILON)
            * gain_v[...]
        ).astype(bf16)
        tok[0, pl.ds(0, block), :] = normed[:, :half_width]
        tok[1, pl.ds(0, block), :] = normed[:, half_width:]
        loads["mixer"].wait()

    with scope("greet"):
        pl.semaphore_wait(barrier, ring + 1)

    def chunk_ref(half, slot, chunk):
        return tok.at[half, pl.ds(place_of(slot, ring) * block + chunk * piece, piece), :]

    def hop(direction, distance, chunk):
        start(
            remote(
                chunk_ref(core, slot_at(direction, distance - 1, ring) % ring, chunk),
                chunk_ref(core, slot_at(direction, distance, ring), chunk),
                ring_send.at[direction, distance, chunk],
                ring_recv.at[direction, distance, chunk],
                ahead if direction == 0 else behind,
            )
        )

    def arrive(distance, chunk):
        for direction in range(2):
            if distance > limit(direction, chunk, ring):
                continue
            here = chunk_ref(core, slot_at(direction, distance, ring), chunk)
            at = (direction, distance, chunk)
            remote(here, here, ring_send.at[at], ring_recv.at[at], sibling).wait_recv()
            if distance < limit(direction, chunk, ring):
                hop(direction, distance + 1, chunk)
            start(remote(here, here, sib_send.at[at], sib_recv.at[at], sibling))

    def swapped(distance):
        for chunk in range(CHUNKS):
            for direction in range(2):
                if distance > limit(direction, chunk, ring):
                    continue
                there = chunk_ref(1 - core, slot_at(direction, distance, ring), chunk)
                at = (direction, distance, chunk)
                remote(there, there, sib_send.at[at], sib_recv.at[at], sibling).wait_recv()

    class Share:
        def __init__(self, view, send, receive):
            self.view, self.send, self.receive = view, send, receive

        def copy(self, owner, i, path, device):
            here = self.view(owner, i)
            return remote(here, here, self.send.at[path, i], self.receive.at[path, i], device)

        def to_across(self, i):
            start(self.copy(part, i, 0, across))

        def to_sibling(self, i):
            start(self.copy(part, i, 1, sibling))

        def both(self, i):
            self.to_across(i)
            self.to_sibling(i)

        def forward(self, i):
            self.copy(across_part, i, 0, sibling).wait_recv()
            start(self.copy(across_part, i, 2, sibling))

        def rest(self, i):
            self.copy(sib_part, i, 1, sibling).wait_recv()
            self.copy(corner_part, i, 2, sibling).wait_recv()

    mixer = Share(
        lambda owner, i: mixer_all.at[owner, pl.ds(i * WINDOW, WINDOW), :], mix_send, mix_recv
    )
    shared = Share(lambda owner, i: shared_all.at[owner], sh_send, sh_recv)
    hidden = Share(
        lambda owner, i: hidden_all.at[owner, pl.ds(place_of(i, ring) * block, block), :],
        hid_send,
        hid_recv,
    )
    att = Share(
        lambda owner, i: att_all.at[owner, pl.ds(i * WINDOW, WINDOW), :], att_send, att_recv
    )

    for chunk in range(CHUNKS):
        for direction in range(2):
            hop(direction, 1, chunk)
    mixer.both(3)
    mixer.both(2)
    mixer.to_sibling(1)
    mixer.to_sibling(0)

    loads["ids"].wait()
    loads["weight"].wait()
    experts = lax.broadcasted_iota(jnp.int32, (ring, block), 0)
    dense = jnp.zeros((ring, block), f32)
    for k in range(TOPK):
        dense = dense + jnp.where(ids_v[k : k + 1, :] == experts, weight_v[k : k + 1, :], 0.0)
    dense_all[0] = dense
    for k in range(1, ring):
        start(
            remote(
                dense_all.at[0], dense_all.at[k], dense_send.at[k], dense_recv.at[k], peers[k - 1]
            )
        )

    def product(first, count, weights, columns):
        lower = tok[0, pl.ds(first, count), :]
        upper = tok[1, pl.ds(first, count), :]
        return jnp.dot(
            lower, weights[pl.ds(0, half_width), columns], preferred_element_type=f32
        ) + jnp.dot(
            upper, weights[pl.ds(half_width, half_width), columns], preferred_element_type=f32
        )

    with scope("c_shared"):
        loads["shared_gate"].wait()
        loads["shared_up"].wait()
        everything = pl.ds(0, shared_width)
        shared_all[part] = (
            jax.nn.silu(product(0, block, shared_gate_v, everything))
            * product(0, block, shared_up_v, everything)
        ).astype(bf16)
        shared.both(0)

    tile = 256

    def compute(slots):
        first = min(place_of(slot, ring) for slot in slots) * block
        count = len(slots) * block

        def one(j, carry):
            columns = pl.ds(pl.multiple_of(j * tile, tile), tile)
            hidden_all[part, pl.ds(first, count), columns] = (
                jax.nn.silu(product(first, count, gate_v, columns))
                * product(first, count, up_v, columns)
            ).astype(bf16)
            return carry

        lax.fori_loop(0, inner // tile, one, 0)
        for slot in slots:
            hidden.both(slot)

    def project(i):
        rows = pl.ds(i * WINDOW, WINDOW)
        mixer.rest(i)
        squares = jnp.zeros((WINDOW, 1), f32)
        for owner in range(parts):
            columns = pl.ds(owner * mixer_cols, mixer_cols)
            value = mixer_all[owner, rows, :].astype(f32)
            squares = squares + jnp.sum(value * value, axis=1, keepdims=True)
            scaled_v[:, columns] = (value * mixer_gain_v[:, columns]).astype(bf16)
        raw = jnp.dot(scaled_v[...], qkv_v[...], preferred_element_type=f32)
        lanes = 2 * HEAD
        heads = heads_v.shape[0]
        gain = query_gain_v[...] * HEAD ** (-0.5)
        gain = jnp.concatenate([gain, gain], axis=1)
        for pair in range(heads // 2):
            two = raw[:, pair * lanes : (pair + 1) * lanes]
            square = two * two
            first_sum = jnp.sum(jnp.where(low, square, 0.0), axis=1, keepdims=True)
            second_sum = jnp.sum(jnp.where(low, 0.0, square), axis=1, keepdims=True)
            inverse = lax.rsqrt(jnp.where(low, first_sum, second_sum) / HEAD + EPSILON)
            two = two * inverse * gain
            heads_v[2 * pair, rows, :] = jnp.where(low, two, 0.0).astype(bf16)
            heads_v[2 * pair + 1, rows, :] = jnp.where(low, 0.0, two).astype(bf16)
        queries_end = heads * HEAD
        second = part // (parts // KV_HEADS)
        mine = low == (second == 0)

        def twice(columns):
            return jnp.where(mine, columns, pltpu.roll(columns, HEAD, 1))

        key = twice(raw[:, queries_end : queries_end + lanes])
        gain = jnp.concatenate([key_gain_v[...], key_gain_v[...]], axis=1)
        key = key * lax.rsqrt(jnp.mean(key * key, axis=1, keepdims=True) + EPSILON) * gain
        val = twice(raw[:, queries_end + lanes : queries_end + 2 * lanes])
        val = val * lax.rsqrt(squares / D + EPSILON)
        band_v[pl.ds(WINDOW + i * WINDOW, WINDOW), :] = jnp.concatenate(
            [key, val], axis=1
        ).astype(bf16)

    halo = band_v.at[pl.ds(0, WINDOW), :]

    def send_halo():
        start(
            remote(
                band_v.at[pl.ds(rows_local, WINDOW), :],
                halo,
                halo_send.at[0],
                halo_recv.at[0],
                ((index + 1) % ring, part),
            )
        )

    def wait_halo():
        remote(halo, halo, halo_send.at[0], halo_recv.at[0], sibling).wait_recv()

    def attend(i):
        rows = pl.ds(i * WINDOW, WINDOW)
        keys = band_v[pl.ds(i * WINDOW, 2 * WINDOW), pl.ds(0, 2 * HEAD)]
        values = band_v[pl.ds(i * WINDOW, 2 * WINDOW), pl.ds(2 * HEAD, 2 * HEAD)]
        bias = bias_v[...]
        if i == 0:
            before = lax.broadcasted_iota(jnp.int32, (WINDOW, 2 * WINDOW), 1) < WINDOW
            bias = jnp.where(before & (index == 0), -jnp.inf, bias)
        mixed = []
        for head in range(heads_v.shape[0]):
            scores = lax.dot_general(
                heads_v[head, rows, :],
                keys,
                (((1,), (1,)), ((), ())),
                preferred_element_type=f32,
            )
            masked = scores + bias
            sink = sink_v[:, head : head + 1]
            peak = jnp.maximum(jnp.max(masked, axis=1, keepdims=True), sink)
            exponent = jnp.exp(masked - peak)
            denominator = jnp.sum(exponent, axis=1, keepdims=True) + jnp.exp(sink - peak)
            probability = (exponent * (1.0 / denominator)).astype(bf16)
            mixed.append(jnp.dot(probability, values, preferred_element_type=f32))
        for pair in range(len(mixed) // 2):
            att_all[part, rows, pl.ds(pair * 2 * HEAD, 2 * HEAD)] = jnp.where(
                low, mixed[2 * pair], mixed[2 * pair + 1]
            ).astype(bf16)

    chip_cols = 2 * out_width

    def spread_columns():
        start(
            remote(
                w_out_hbm.at[:, pl.ds(pl.multiple_of(sib_part * out_width, out_width), out_width)],
                out_cols.at[part],
                wcol_send.at[0],
                wcol_recv.at[0],
                sibling,
            )
        )
        mine = pl.ds(pl.multiple_of(index * share_rows, share_rows), share_rows)
        start(
            remote(
                w_out_hbm.at[
                    mine, pl.ds(pl.multiple_of((1 - far) * chip_cols, chip_cols), chip_cols)
                ],
                out_stage.at[mine, :],
                wcol_send.at[1],
                wcol_recv.at[1],
                across,
            )
        )

    def stage_ref(slot, chunk):
        owner = peer_index[(ring - slot) % ring]
        first = owner * share_rows + chunk * share_piece
        return out_stage.at[pl.ds(pl.multiple_of(first, share_piece), share_piece), :]

    def column_hop(direction, distance, chunk):
        here = stage_ref(slot_at(direction, distance - 1, ring) % ring, chunk)
        at = (direction, distance, chunk)
        start(
            remote(
                here,
                here,
                wring_send.at[at],
                wring_recv.at[at],
                ahead if direction == 0 else behind,
            )
        )

    def column_start():
        mine = out_stage.at[pl.ds(pl.multiple_of(index * share_rows, share_rows), share_rows), :]
        remote(mine, mine, wcol_send.at[1], wcol_recv.at[1], across).wait_recv()
        for chunk in range(CHUNKS):
            for direction in range(2):
                column_hop(direction, 1, chunk)

    def column_arrive(distance):
        for chunk in range(CHUNKS):
            for direction in range(2):
                if distance > limit(direction, chunk, ring):
                    continue
                here = stage_ref(slot_at(direction, distance, ring), chunk)
                at = (direction, distance, chunk)
                remote(here, here, wring_send.at[at], wring_recv.at[at], sibling).wait_recv()
                if distance < limit(direction, chunk, ring):
                    column_hop(direction, distance + 1, chunk)

    def column_swap():
        start(
            remote(
                out_stage.at[
                    :, pl.ds(pl.multiple_of((1 - core) * out_width, out_width), out_width)
                ],
                out_cols.at[across_part],
                wcol_send.at[2],
                wcol_recv.at[2],
                sibling,
            )
        )

    def column_wait():
        loads["out_own"].wait()
        for i, owner in ((0, sib_part), (2, corner_part)):
            here = out_cols.at[owner]
            remote(here, here, wcol_send.at[i], wcol_recv.at[i], sibling).wait_recv()

    def finish_mixer(i):
        rows = pl.ds(i * WINDOW, WINDOW)
        att.rest(i)
        total = jnp.dot(
            att_all[across_part, rows, :],
            out_stage[:, pl.ds(pl.multiple_of(core * out_width, out_width), out_width)],
            preferred_element_type=f32,
        )
        for owner in (part, sib_part, corner_part):
            total = total + jnp.dot(
                att_all[owner, rows, :], out_cols[owner], preferred_element_type=f32
            )
        mixer_v[rows, :] = total.astype(bf16)
        stores.append(
            pltpu.make_async_copy(mixer_v.at[rows, :], mixer_result.at[rows, :], store_sem.at[i])
        )
        stores[-1].start()

    diagonal = lax.broadcasted_iota(jnp.int32, (block, block), 0) == lax.broadcasted_iota(
        jnp.int32, (block, block), 1
    )

    def weight_column(slot):
        row = dense_all[slot, pl.ds(index, 1), :]
        return jnp.sum(jnp.where(diagonal, row, 0.0), axis=1, keepdims=True)

    def weighted(slots):
        for slot in slots:
            hidden.rest(slot)
        first = min(place_of(slot, ring) for slot in slots) * block
        count = len(slots) * block
        total = jnp.dot(
            hidden_all[0, pl.ds(first, count), :],
            down_v[pl.ds(0, inner), :],
            preferred_element_type=f32,
        )
        for owner in range(1, parts):
            total = total + jnp.dot(
                hidden_all[owner, pl.ds(first, count), :],
                down_v[pl.ds(owner * inner, inner), :],
                preferred_element_type=f32,
            )
        rounded = total.astype(bf16).astype(f32)
        ordered = sorted(slots, key=lambda slot: place_of(slot, ring))
        ready[pl.ds(first, count), :] = rounded * jnp.concatenate(
            [weight_column(slot) for slot in ordered], axis=0
        )

    def own_rows():
        weighted([0])
        shared.rest(0)
        own = ready[pl.ds(0, block), :]
        for owner in range(parts):
            own = own + jnp.dot(
                shared_all[owner],
                shared_down_v[pl.ds(owner * shared_width, shared_width), :],
                preferred_element_type=f32,
            )
        ready[pl.ds(0, block), :] = own

    back_rows = block // PARTS_BACK

    def longest(direction, part_back):
        return limit(direction, part_back * CHUNKS // PARTS_BACK, ring)

    def back_wait(direction, distance, b):
        here = coming.at[direction, distance, pl.ds(b * back_rows, back_rows), :]
        at = (direction, distance, b)
        remote(here, here, back_send.at[at], back_recv.at[at], ahead).wait_recv()
        return here[...].astype(f32)

    def push(distance, final):
        for b in range(PARTS_BACK):
            for direction in range(2):
                if longest(direction, b) != final:
                    continue
                slot = slot_at(1 - direction, distance, ring)
                first = place_of(slot, ring) * block + b * back_rows
                value = ready[pl.ds(first, back_rows), :]
                if distance < final:
                    value = value + back_wait(direction, distance + 1, b)
                rows = pl.ds(b * back_rows, back_rows)
                going[direction, distance, rows, :] = value.astype(bf16)
                at = (direction, distance, b)
                start(
                    remote(
                        going.at[direction, distance, rows, :],
                        coming.at[direction, distance, rows, :],
                        back_send.at[at],
                        back_recv.at[at],
                        ahead if direction == 0 else behind,
                    )
                )

    def finish_expert(b):
        rows = pl.ds(b * back_rows, back_rows)
        expert_v[rows, :] = (
            ready[rows, :] + back_wait(0, 1, b) + back_wait(1, 1, b)
        ).astype(bf16)

    with scope("c_h0"):
        loads["gate"].wait()
        loads["up"].wait()
        compute([0])
    spread_columns()
    with scope("A1c0"):
        arrive(1, 0)
    with scope("fwd_m3"):
        mixer.forward(3)
    with scope("A1c1"):
        arrive(1, 1)
    with scope("fwd_m2"):
        mixer.forward(2)
    with scope("S1"):
        swapped(1)
    with scope("c_h1"):
        compute([1, ring - 1])
    with scope("A2c0"):
        arrive(2, 0)
    with scope("w_qkv"):
        for name in ("mixer_gain", "query_gain", "key_gain", "sink", "query", "key", "value"):
            loads[name].wait()
    with scope("qkv3"):
        project(3)
        send_halo()
    with scope("qkv2"):
        project(2)
    with scope("A2c1"):
        arrive(2, 1)
    with scope("S2"):
        swapped(2)
    with scope("c_h2"):
        compute([2, ring - 2])
    with scope("A3c0"):
        arrive(3, 0)
    with scope("att3"):
        attend(3)
        att.to_sibling(3)
    with scope("fwd_sh_h0"):
        shared.forward(0)
        hidden.forward(0)
    with scope("A3c1"):
        arrive(3, 1)
    with scope("S3"):
        swapped(3)
    with scope("c_h3"):
        compute([3, ring - 3])
    with scope("A4"):
        arrive(4, 0)
        arrive(4, 1)
    with scope("w0"):
        column_start()
    with scope("fwd_h1"):
        hidden.forward(1)
        hidden.forward(ring - 1)
    with scope("S4"):
        swapped(4)
    with scope("c_h4"):
        compute([4])
    mixer.to_across(1)
    att.to_across(3)
    mixer.to_across(0)
    with scope("own"):
        loads["down"].wait()
        loads["shared_down"].wait()
        for peer in range(1, ring):
            here = dense_all.at[peer]
            remote(here, here, dense_send.at[peer], dense_recv.at[peer], sibling).wait_recv()
        own_rows()
    with scope("w1"):
        column_arrive(1)
    with scope("down1"):
        weighted([1, ring - 1])
    with scope("fwd_h2"):
        hidden.forward(2)
        hidden.forward(ring - 2)
    with scope("w2"):
        column_arrive(2)
    with scope("down2"):
        weighted([2, ring - 2])
    with scope("w3"):
        column_arrive(3)
    with scope("fwd_h3"):
        hidden.forward(3)
        hidden.forward(ring - 3)
    with scope("down3"):
        weighted([3, ring - 3])
        push(3, 3)
    with scope("w4"):
        column_arrive(4)
        column_swap()
    with scope("fwd_h4"):
        hidden.forward(4)
    with scope("down4"):
        weighted([4])
        push(4, 4)
    with scope("fwd_m1"):
        mixer.forward(1)
    with scope("push2_3"):
        push(2, 3)
    with scope("qkv1"):
        project(1)
    with scope("att2"):
        attend(2)
        att.both(2)
    with scope("push3_4"):
        push(3, 4)
    with scope("fwd_a3m0"):
        att.forward(3)
        mixer.forward(0)
    with scope("halo"):
        wait_halo()
    with scope("push1_3"):
        push(1, 3)
    with scope("qkv0"):
        project(0)
    with scope("att1"):
        attend(1)
        att.both(1)
    with scope("att0"):
        attend(0)
        att.both(0)
    with scope("push2_4"):
        push(2, 4)
    with scope("fwd_a2"):
        att.forward(2)
    with scope("out3"):
        column_wait()
        finish_mixer(3)
    with scope("push1_4"):
        push(1, 4)
    with scope("fwd_a10"):
        att.forward(1)
        att.forward(0)
    with scope("out21"):
        finish_mixer(2)
        finish_mixer(1)
    with scope("out0"):
        finish_mixer(0)
    with scope("fin_exp"):
        for b in range(PARTS_BACK):
            finish_expert(b)
        stores.append(pltpu.make_async_copy(expert_v, expert_result, store_sem.at[pieces]))
        stores[-1].start()
    with scope("w_end"):
        for copy in stores:
            copy.wait()
        for copy in pending:
            copy.wait_send()


def shards(
    mixer_input,
    mixer_gain,
    w_query,
    w_key,
    w_value,
    query_gain,
    key_gain,
    sink_logit,
    w_output,
    expert_input,
    expert_gain,
    route_ids,
    route_weight,
    expert_gate,
    expert_up,
    expert_down,
    shared_gate,
    shared_up,
    shared_down,
):
    ring = lax.axis_size("ep")
    parts = lax.axis_size("tp")
    rows_local, mixer_cols = mixer_input.shape
    tokens_local, width = expert_input.shape
    hidden_width = expert_gate.shape[2]
    shared_width = shared_gate.shape[1]
    out_width = expert_down.shape[2]
    head_width = w_query.shape[1]
    pieces = rows_local // WINDOW
    half = ring // 2
    hbm = pl.BlockSpec(memory_space=pl.ANY)
    bf16, f32 = jnp.bfloat16, jnp.float32
    vm = pltpu.VMEM

    def sems(*shape):
        return [pltpu.SemaphoreType.DMA(shape)] * 2

    outputs = pl.pallas_call(
        functools.partial(layer_kernel, ring),
        out_shape=(
            jax.ShapeDtypeStruct((rows_local, out_width), bf16),
            jax.ShapeDtypeStruct((tokens_local, out_width), bf16),
        ),
        in_specs=[hbm] * 19,
        out_specs=(hbm,) * 2,
        scratch_shapes=[
            vm((tokens_local, width), bf16),
            vm((1, width), f32),
            vm((TOPK, tokens_local), jnp.int32),
            vm((TOPK, tokens_local), f32),
            vm((1, parts * mixer_cols), f32),
            vm((1, HEAD), f32),
            vm((1, HEAD), f32),
            vm((1, sink_logit.shape[0]), f32),
            vm((parts, rows_local, mixer_cols), bf16),
            vm((parts, ring * tokens_local, hidden_width), bf16),
            vm((parts, tokens_local, shared_width), bf16),
            vm((parts, rows_local, head_width), bf16),
            vm((ring, ring, tokens_local), f32),
            vm((2, ring * tokens_local, width // 2), bf16),
            vm((width, hidden_width), bf16),
            vm((width, hidden_width), bf16),
            vm((width, shared_width), bf16),
            vm((width, shared_width), bf16),
            vm((width, head_width + w_key.shape[1] + w_value.shape[1]), bf16),
            vm(expert_down.shape[1:], bf16),
            vm(shared_down.shape, bf16),
            vm((parts, head_width, out_width), bf16),
            vm((head_width, 2 * out_width), bf16),
            vm((WINDOW, parts * mixer_cols), bf16),
            vm((head_width // HEAD, rows_local, 2 * HEAD), bf16),
            vm((WINDOW + rows_local, 4 * HEAD), bf16),
            vm((WINDOW, 2 * WINDOW), f32),
            vm((ring * tokens_local, out_width), f32),
            vm((2, half + 1, tokens_local, out_width), bf16),
            vm((2, half + 1, tokens_local, out_width), bf16),
            vm((rows_local, out_width), bf16),
            vm((tokens_local, out_width), bf16),
            pltpu.SemaphoreType.DMA((19,)),
            pltpu.SemaphoreType.DMA((pieces + 1,)),
            *sems(2, half + 1, CHUNKS),
            *sems(2, half + 1, CHUNKS),
            *sems(3, pieces),
            *sems(3, ring),
            *sems(3, 1),
            *sems(3, pieces),
            *sems(ring),
            *sems(1),
            *sems(3),
            *sems(2, half + 1, CHUNKS),
            *sems(2, half + 1, PARTS_BACK),
        ],
        compiler_params=pltpu.CompilerParams(
            collective_id=0, has_side_effects=True, vmem_limit_bytes=VMEM_LIMIT
        ),
        name="layer",
    )(
        expert_input,
        expert_gain[None, :],
        route_ids.T,
        route_weight.T,
        mixer_input,
        mixer_gain[None, :],
        query_gain[None, :],
        key_gain[None, :],
        sink_logit[None, :],
        expert_gate[0],
        expert_up[0],
        shared_gate,
        shared_up,
        w_query,
        w_key,
        w_value,
        w_output,
        expert_down[0],
        shared_down,
    )
    return outputs


def plan(*arrays):
    route_ids = arrays[11]
    capacity = 2 * route_ids.size // lax.axis_size("ep")
    whole_blocks = capacity >= route_ids.shape[0]
    if whole_blocks and lax.axis_size("tp") == 4:
        return shards(*arrays)
    return shards_routed(*arrays)


def solution(mesh):
    in_specs = (
        P("ep", "tp"),
        P(),
        P(None, "tp"),
        P(),
        P(),
        P(),
        P(),
        P("tp"),
        P("tp", None),
        P("ep", None),
        P(),
        P("ep", None),
        P("ep", None),
        P("ep", None, "tp"),
        P("ep", None, "tp"),
        P("ep", None, "tp"),
        P(None, "tp"),
        P(None, "tp"),
        P(None, "tp"),
    )
    out_specs = (P("ep", "tp"), P("ep", "tp"))
    return jax.shard_map(plan, mesh=mesh, in_specs=in_specs, out_specs=out_specs, check_vma=False)
```

time: 77.2 us -> 67.9 us (0.88)
  Pallas kernels: 70 us -> 63.6 us
  local copies, waits for them, and re-layouts: 5.02 us -> 3.44 us
  other arithmetic: 1.3 us -> 0 us
    pallas_call x1, Pallas kernels: 70 us -> 63.6 us  [shards(): pl.pallas_call(functools.partial(layer_kernel, ring), out_shape=(jax.Shap...]
    reduce_sum x1 -> x0, other arithmetic: 1.3 us -> none  [shards(): dense = jnp.sum(jnp.where(chosen, route_weight[:, :, None], 0.0), axis=1).T]
    another operation x1 -> x0, local copies, waits for them, and re-layouts: 0.86 us -> none  [shards(): jnp.repeat(sink_logit, WINDOW)[:, None]]
where the time goes in v1:
time: 67.9 us; the launch traced here: 67.7 us
  Pallas kernels  63.6 us (94%)
  local copies, waits for them, and re-layouts  3.44 us (5%)
    pallas_call x1, Pallas kernels, shards(): pl.pallas_call(functools.partial(layer_kernel, ring), out_shape=(jax.Shap...  63.6 us
    unnamed x2, local copies, waits for them, and re-layouts  3.44 us

profile of v1, /device:TPU:0, one launch (start us, length us, event | category | flops | bytes accessed | tf_op | source)
XLA Modules:
  0.0 67.7 jit_solution(134364241910591173)
XLA Ops:
  0.6 63.6 %layer.1 = (bf16[512,512]{1,0:T(8,128)(2,1)}, bf16[128,512]{1,0:T(8,128)(2,1)}) custom-call(bf16[128,2048]{1,0:T(8,128)(2,1)} %rows_hbm.1, f32[1,2048]{1,0:T(1,128)} %bitcast.13, s32[4,128]{1,0:T(4,128)} %bitcast.15, f32[4,128]{1,0:T(4,128)} %bitcast.16, bf16[512,512]{1,0:T(8,128)(2,1)} %mixer_hbm.1, f32[1,2048]{1,0:T(1,128)} %bitcast.14, f32[1,64]{1,0:T(1,128)} %bitcast.17, ...), custom_call_target="tpu_custom_call" | custom-call | tf_op jit(solution)/shard_map/layer/pallas_call | solution.py:979
  64.2 1.9 %copy.23 = bf16[512,512]{1,0:T(8,128)(2,1)} copy(bf16[512,512]{1,0:T(8,128)(2,1)} %get-tuple-element.4) | data formatting | bytes 1048576
  66.1 1.6 %copy.24 = bf16[128,512]{1,0:T(8,128)(2,1)} copy(bf16[128,512]{1,0:T(8,128)(2,1)} %get-tuple-element.5) | data formatting | bytes 262144

commit v2 on v1

--- a/solution.py
+++ b/solution.py
@@ -279,9 +279,8 @@
     expert_v,
     load_sem,
     store_sem,
-    ring_send,
+    tok_send,
     ring_recv,
-    sib_send,
     sib_recv,
     mix_send,
     mix_recv,
@@ -325,23 +324,25 @@
     shared_width = shared_all.shape[2]
     head_rows = out_cols.shape[1]
     share_rows = head_rows // ring
-    share_piece = share_rows // CHUNKS
 
     barrier = pltpu.get_barrier_semaphore()
     for device in peers + [sibling, across]:
         pl.semaphore_signal(barrier, inc=1, device_id=device, device_id_type=pl.DeviceIdType.MESH)
 
-    pending, stores = [], []
+    stores = []
 
     def start(copy):
         copy.start()
-        pending.append(copy)
 
     loads = {}
 
     def load(name, source, target):
         loads[name] = pltpu.make_async_copy(source, target, load_sem.at[len(loads)])
         loads[name].start()
+
+    def load_qkv(source, first):
+        target = qkv_v.at[:, pl.ds(first, source.shape[1])]
+        pltpu.make_async_copy(source, target, load_sem.at[len(loads)]).start()
 
     own_cols = pl.ds(pl.multiple_of(part * out_width, out_width), out_width)
     load("rows", rows_hbm, rows_v)
@@ -357,13 +358,11 @@
     load("query_gain", query_gain_hbm, query_gain_v)
     load("key_gain", key_gain_hbm, key_gain_v)
     load("sink", sink_hbm, sink_v)
-    load("query", query_hbm, qkv_v.at[:, pl.ds(0, query_hbm.shape[1])])
-    load("key", key_hbm, qkv_v.at[:, pl.ds(query_hbm.shape[1], key_hbm.shape[1])])
-    load(
-        "value",
-        value_hbm,
-        qkv_v.at[:, pl.ds(query_hbm.shape[1] + key_hbm.shape[1], value_hbm.shape[1])],
-    )
+    query_cols, key_cols = query_hbm.shape[1], key_hbm.shape[1]
+    load_qkv(query_hbm, 0)
+    load_qkv(key_hbm, query_cols)
+    load_qkv(value_hbm, query_cols + key_cols)
+    loads["qkv"] = pltpu.make_async_copy(qkv_v, qkv_v, load_sem.at[len(loads)])
     load("out_own", w_out_hbm.at[:, own_cols], out_cols.at[part])
     load("down", down_hbm, down_v)
     load("shared_down", shared_down_hbm, shared_down_v)
@@ -400,31 +399,28 @@
             remote(
                 chunk_ref(core, slot_at(direction, distance - 1, ring) % ring, chunk),
                 chunk_ref(core, slot_at(direction, distance, ring), chunk),
-                ring_send.at[direction, distance, chunk],
-                ring_recv.at[direction, distance, chunk],
+                tok_send.at[0],
+                ring_recv.at[direction, distance - 1, chunk],
                 ahead if direction == 0 else behind,
             )
         )
 
-    def arrive(distance, chunk):
+    def arrive(distance, k):
         for direction in range(2):
+            chunk = k if direction == 0 else CHUNKS - 1 - k
             if distance > limit(direction, chunk, ring):
                 continue
             here = chunk_ref(core, slot_at(direction, distance, ring), chunk)
-            at = (direction, distance, chunk)
-            remote(here, here, ring_send.at[at], ring_recv.at[at], sibling).wait_recv()
+            got = ring_recv.at[direction, distance - 1, chunk]
+            remote(here, here, tok_send.at[0], got, sibling).wait_recv()
             if distance < limit(direction, chunk, ring):
                 hop(direction, distance + 1, chunk)
-            start(remote(here, here, sib_send.at[at], sib_recv.at[at], sibling))
+            start(remote(here, here, tok_send.at[0], sib_recv.at[distance - 1], sibling))
 
     def swapped(distance):
-        for chunk in range(CHUNKS):
-            for direction in range(2):
-                if distance > limit(direction, chunk, ring):
-                    continue
-                there = chunk_ref(1 - core, slot_at(direction, distance, ring), chunk)
-                at = (direction, distance, chunk)
-                remote(there, there, sib_send.at[at], sib_recv.at[at], sibling).wait_recv()
+        count = 2 if distance < steps else 1
+        there = tok.at[1 - core, pl.ds((2 * distance - 1) * block, count * block), :]
+        remote(there, there, tok_send.at[0], sib_recv.at[distance - 1], sibling).wait_recv()
 
     class Share:
         def __init__(self, view, send, receive):
@@ -432,7 +428,7 @@
 
         def copy(self, owner, i, path, device):
             here = self.view(owner, i)
-            return remote(here, here, self.send.at[path, i], self.receive.at[path, i], device)
+            return remote(here, here, self.send.at[0], self.receive.at[path, i], device)
 
         def to_across(self, i):
             start(self.copy(part, i, 0, across))
@@ -446,11 +442,10 @@
 
         def forward(self, i):
             self.copy(across_part, i, 0, sibling).wait_recv()
-            start(self.copy(across_part, i, 2, sibling))
+            start(self.copy(across_part, i, 1, sibling))
 
         def rest(self, i):
-            self.copy(sib_part, i, 1, sibling).wait_recv()
-            self.copy(corner_part, i, 2, sibling).wait_recv()
+            self.copy(pl.ds(0, 2), i, 1, sibling).wait_recv()
 
     mixer = Share(
         lambda owner, i: mixer_all.at[owner, pl.ds(i * WINDOW, WINDOW), :], mix_send, mix_recv
@@ -465,9 +460,9 @@
         lambda owner, i: att_all.at[owner, pl.ds(i * WINDOW, WINDOW), :], att_send, att_recv
     )
 
-    for chunk in range(CHUNKS):
+    for k in range(CHUNKS):
         for direction in range(2):
-            hop(direction, 1, chunk)
+            hop(direction, 1, k if direction == 0 else CHUNKS - 1 - k)
     mixer.both(3)
     mixer.both(2)
     mixer.to_sibling(1)
@@ -483,7 +478,7 @@
     for k in range(1, ring):
         start(
             remote(
-                dense_all.at[0], dense_all.at[k], dense_send.at[k], dense_recv.at[k], peers[k - 1]
+                dense_all.at[0], dense_all.at[k], dense_send.at[0], dense_recv.at[0], peers[k - 1]
             )
         )
 
@@ -632,41 +627,15 @@
             )
         )
 
-    def stage_ref(slot, chunk):
-        owner = peer_index[(ring - slot) % ring]
-        first = owner * share_rows + chunk * share_piece
-        return out_stage.at[pl.ds(pl.multiple_of(first, share_piece), share_piece), :]
-
-    def column_hop(direction, distance, chunk):
-        here = stage_ref(slot_at(direction, distance - 1, ring) % ring, chunk)
-        at = (direction, distance, chunk)
-        start(
-            remote(
-                here,
-                here,
-                wring_send.at[at],
-                wring_recv.at[at],
-                ahead if direction == 0 else behind,
-            )
-        )
-
     def column_start():
         mine = out_stage.at[pl.ds(pl.multiple_of(index * share_rows, share_rows), share_rows), :]
         remote(mine, mine, wcol_send.at[1], wcol_recv.at[1], across).wait_recv()
-        for chunk in range(CHUNKS):
-            for direction in range(2):
-                column_hop(direction, 1, chunk)
-
-    def column_arrive(distance):
-        for chunk in range(CHUNKS):
-            for direction in range(2):
-                if distance > limit(direction, chunk, ring):
-                    continue
-                here = stage_ref(slot_at(direction, distance, ring), chunk)
-                at = (direction, distance, chunk)
-                remote(here, here, wring_send.at[at], wring_recv.at[at], sibling).wait_recv()
-                if distance < limit(direction, chunk, ring):
-                    column_hop(direction, distance + 1, chunk)
+        for device in peers:
+            start(remote(mine, mine, wring_send.at[0], wring_recv.at[0], device))
+
+    def column_rest():
+        here = out_stage.at[pl.ds(0, (ring - 1) * share_rows), :]
+        remote(here, here, wring_send.at[0], wring_recv.at[0], sibling).wait_recv()
 
     def column_swap():
         start(
@@ -754,44 +723,55 @@
 
     def back_wait(direction, distance, b):
         here = coming.at[direction, distance, pl.ds(b * back_rows, back_rows), :]
-        at = (direction, distance, b)
-        remote(here, here, back_send.at[at], back_recv.at[at], ahead).wait_recv()
+        got = back_recv.at[direction, distance - 1, b]
+        remote(here, here, back_send.at[0], got, ahead).wait_recv()
         return here[...].astype(f32)
 
-    def push(distance, final):
+    def push(distance, long, directions=(0, 1)):
         for b in range(PARTS_BACK):
-            for direction in range(2):
-                if longest(direction, b) != final:
+            for direction in directions:
+                if (longest(direction, b) == steps) != long:
                     continue
                 slot = slot_at(1 - direction, distance, ring)
                 first = place_of(slot, ring) * block + b * back_rows
                 value = ready[pl.ds(first, back_rows), :]
-                if distance < final:
+                hops = 1
+                if long and distance == steps:
+                    hops = 2
+                elif long and distance == steps - 2:
+                    hops = 2
+                    value = value + back_wait(direction, distance + 1, b)
+                    value = value + back_wait(direction, distance + 2, b)
+                elif not long and distance < steps - 1:
                     value = value + back_wait(direction, distance + 1, b)
                 rows = pl.ds(b * back_rows, back_rows)
-                going[direction, distance, rows, :] = value.astype(bf16)
-                at = (direction, distance, b)
+                at = direction * steps + distance - 1
+                going[at, rows, :] = value.astype(bf16)
                 start(
                     remote(
-                        going.at[direction, distance, rows, :],
+                        going.at[at, rows, :],
                         coming.at[direction, distance, rows, :],
-                        back_send.at[at],
-                        back_recv.at[at],
-                        ahead if direction == 0 else behind,
+                        back_send.at[0],
+                        back_recv.at[direction, distance - 1, b],
+                        peers[hops - 1 if direction == 0 else -hops],
                     )
                 )
 
     def finish_expert(b):
         rows = pl.ds(b * back_rows, back_rows)
-        expert_v[rows, :] = (
-            ready[rows, :] + back_wait(0, 1, b) + back_wait(1, 1, b)
-        ).astype(bf16)
+        total = ready[rows, :]
+        for direction in range(2):
+            total = total + back_wait(direction, 1, b)
+            if longest(direction, b) == steps:
+                total = total + back_wait(direction, 2, b)
+        expert_v[rows, :] = total.astype(bf16)
 
     with scope("c_h0"):
         loads["gate"].wait()
         loads["up"].wait()
         compute([0])
     spread_columns()
+    mixer.to_across(1)
     with scope("A1c0"):
         arrive(1, 0)
     with scope("fwd_m3"):
@@ -800,142 +780,153 @@
         arrive(1, 1)
     with scope("fwd_m2"):
         mixer.forward(2)
+    with scope("w_qkv"):
+        for name in ("mixer_gain", "query_gain", "key_gain", "sink", "qkv"):
+            loads[name].wait()
+    with scope("qkv3"):
+        project(3)
+        send_halo()
     with scope("S1"):
         swapped(1)
     with scope("c_h1"):
         compute([1, ring - 1])
     with scope("A2c0"):
         arrive(2, 0)
-    with scope("w_qkv"):
-        for name in ("mixer_gain", "query_gain", "key_gain", "sink", "query", "key", "value"):
-            loads[name].wait()
-    with scope("qkv3"):
-        project(3)
-        send_halo()
     with scope("qkv2"):
         project(2)
+    with scope("att3"):
+        attend(3)
+        att.to_sibling(3)
     with scope("A2c1"):
         arrive(2, 1)
+    with scope("fwd_sh_h0"):
+        shared.forward(0)
+        hidden.forward(0)
     with scope("S2"):
         swapped(2)
     with scope("c_h2"):
         compute([2, ring - 2])
     with scope("A3c0"):
         arrive(3, 0)
-    with scope("att3"):
-        attend(3)
-        att.to_sibling(3)
-    with scope("fwd_sh_h0"):
-        shared.forward(0)
-        hidden.forward(0)
+    with scope("fwd_m1"):
+        mixer.forward(1)
+    with scope("own"):
+        loads["down"].wait()
+        loads["shared_down"].wait()
+        here = dense_all.at[pl.ds(1, ring - 1)]
+        remote(here, here, dense_send.at[0], dense_recv.at[0], sibling).wait_recv()
+        own_rows()
+    with scope("qkv1"):
+        project(1)
     with scope("A3c1"):
         arrive(3, 1)
+    with scope("w0"):
+        column_start()
+    with scope("fwd_h1"):
+        hidden.forward(1)
     with scope("S3"):
         swapped(3)
     with scope("c_h3"):
         compute([3, ring - 3])
     with scope("A4"):
         arrive(4, 0)
-        arrive(4, 1)
-    with scope("w0"):
-        column_start()
-    with scope("fwd_h1"):
-        hidden.forward(1)
+    with scope("fwd_h7"):
         hidden.forward(ring - 1)
+    with scope("att2"):
+        attend(2)
+        att.to_sibling(2)
     with scope("S4"):
         swapped(4)
     with scope("c_h4"):
         compute([4])
-    mixer.to_across(1)
+    mixer.to_across(0)
     att.to_across(3)
-    mixer.to_across(0)
-    with scope("own"):
-        loads["down"].wait()
-        loads["shared_down"].wait()
-        for peer in range(1, ring):
-            here = dense_all.at[peer]
-            remote(here, here, dense_send.at[peer], dense_recv.at[peer], sibling).wait_recv()
-        own_rows()
-    with scope("w1"):
-        column_arrive(1)
+    att.to_across(2)
     with scope("down1"):
         weighted([1, ring - 1])
+    push(1, True)
     with scope("fwd_h2"):
         hidden.forward(2)
         hidden.forward(ring - 2)
-    with scope("w2"):
-        column_arrive(2)
+    with scope("halo"):
+        wait_halo()
+    with scope("fwd_h3"):
+        hidden.forward(3)
     with scope("down2"):
         weighted([2, ring - 2])
-    with scope("w3"):
-        column_arrive(3)
-    with scope("fwd_h3"):
-        hidden.forward(3)
+    with scope("down3"):
+        weighted([3])
+        push(3, False, (1,))
+        push(3, True, (1,))
+    with scope("fwd_h5"):
         hidden.forward(ring - 3)
-    with scope("down3"):
-        weighted([3, ring - 3])
-        push(3, 3)
-    with scope("w4"):
-        column_arrive(4)
+    with scope("col_rest"):
+        column_rest()
         column_swap()
+    with scope("down5"):
+        weighted([ring - 3])
+        push(3, False, (0,))
+        push(3, True, (0,))
     with scope("fwd_h4"):
         hidden.forward(4)
     with scope("down4"):
         weighted([4])
-        push(4, 4)
-    with scope("fwd_m1"):
-        mixer.forward(1)
-    with scope("push2_3"):
-        push(2, 3)
-    with scope("qkv1"):
-        project(1)
-    with scope("att2"):
-        attend(2)
-        att.both(2)
-    with scope("push3_4"):
-        push(3, 4)
-    with scope("fwd_a3m0"):
-        att.forward(3)
+        push(4, True)
+    with scope("fwd_m0"):
         mixer.forward(0)
-    with scope("halo"):
-        wait_halo()
-    with scope("push1_3"):
-        push(1, 3)
+    with scope("push2s"):
+        push(2, False)
     with scope("qkv0"):
         project(0)
     with scope("att1"):
         attend(1)
         att.both(1)
+    with scope("push2l"):
+        push(2, True)
+    with scope("push1s"):
+        push(1, False)
     with scope("att0"):
         attend(0)
         att.both(0)
-    with scope("push2_4"):
-        push(2, 4)
-    with scope("fwd_a2"):
+    with scope("fwd_a32"):
+        att.forward(3)
         att.forward(2)
+    with scope("fwd_a1"):
+        att.forward(1)
     with scope("out3"):
         column_wait()
         finish_mixer(3)
-    with scope("push1_4"):
-        push(1, 4)
-    with scope("fwd_a10"):
-        att.forward(1)
-        att.forward(0)
-    with scope("out21"):
+    with scope("out2"):
         finish_mixer(2)
-        finish_mixer(1)
-    with scope("out0"):
-        finish_mixer(0)
     with scope("fin_exp"):
         for b in range(PARTS_BACK):
             finish_expert(b)
         stores.append(pltpu.make_async_copy(expert_v, expert_result, store_sem.at[pieces]))
         stores[-1].start()
+    with scope("fwd_a0"):
+        att.forward(0)
+    with scope("out1"):
+        finish_mixer(1)
+    with scope("out0"):
+        finish_mixer(0)
     with scope("w_end"):
         for copy in stores:
             copy.wait()
-        for copy in pending:
-            copy.wait_send()
+        for ref, send in (
+            (tok.at[:, pl.ds(0, (ring - 1) * block), :], tok_send.at[0]),
+            (mixer_all.at[pl.ds(0, parts - 1)], mix_send.at[0]),
+            (hidden_all.at[pl.ds(0, parts - 1)], hid_send.at[0]),
+            (shared_all.at[pl.ds(0, parts - 1)], sh_send.at[0]),
+            (att_all.at[pl.ds(0, parts - 1)], att_send.at[0]),
+            (dense_all.at[pl.ds(0, ring - 1)], dense_send.at[0]),
+            (halo, halo_send.at[0]),
+            (out_cols.at[part], wcol_send.at[0]),
+            (out_stage.at[pl.ds(0, share_rows), :], wcol_send.at[1]),
+            (out_cols.at[part], wcol_send.at[2]),
+            (out_stage.at[pl.ds(0, (ring - 1) * share_rows), :], wring_send.at[0]),
+            (going.at[pl.ds(0, ring - 1)], back_send.at[0]),
+        ):
+            remote(ref, ref, send, halo_recv.at[0], sibling).wait_send()
 
 
 def shards(
@@ -973,9 +964,7 @@
     bf16, f32 = jnp.bfloat16, jnp.float32
     vm = pltpu.VMEM
 
-    def sems(*shape):
-        return [pltpu.SemaphoreType.DMA(shape)] * 2
-
+    dma = pltpu.SemaphoreType.DMA
     outputs = pl.pallas_call(
         functools.partial(layer_kernel, ring),
         out_shape=(
@@ -1013,23 +1002,33 @@
             vm((WINDOW + rows_local, 4 * HEAD), bf16),
             vm((WINDOW, 2 * WINDOW), f32),
             vm((ring * tokens_local, out_width), f32),
-            vm((2, half + 1, tokens_local, out_width), bf16),
+            vm((2 * half, tokens_local, out_width), bf16),
             vm((2, half + 1, tokens_local, out_width), bf16),
             vm((rows_local, out_width), bf16),
             vm((tokens_local, out_width), bf16),
-            pltpu.SemaphoreType.DMA((19,)),
-            pltpu.SemaphoreType.DMA((pieces + 1,)),
-            *sems(2, half + 1, CHUNKS),
-            *sems(2, half + 1, CHUNKS),
-            *sems(3, pieces),
-            *sems(3, ring),
-            *sems(3, 1),
-            *sems(3, pieces),
-            *sems(ring),
-            *sems(1),
-            *sems(3),
-            *sems(2, half + 1, CHUNKS),
-            *sems(2, half + 1, PARTS_BACK),
+            dma((17,)),
+            dma((pieces + 1,)),
+            dma((1,)),
+            dma((2, half, CHUNKS)),
+            dma((half,)),
+            dma((1,)),
+            dma((2, pieces)),
+            dma((1,)),
+            dma((2, ring)),
+            dma((1,)),
+            dma((2, 1)),
+            dma((1,)),
+            dma((2, pieces)),
+            dma((1,)),
+            dma((1,)),
+            dma((1,)),
+            dma((1,)),
+            dma((3,)),
+            dma((3,)),
+            dma((1,)),
+            dma((1,)),
+            dma((1,)),
+            dma((2, half, PARTS_BACK)),
         ],
         compiler_params=pltpu.CompilerParams(
             collective_id=0, has_side_effects=True, vmem_limit_bytes=VMEM_LIMIT
@@ -1063,7 +1062,8 @@
     route_ids = arrays[11]
     capacity = 2 * route_ids.size // lax.axis_size("ep")
     whole_blocks = capacity >= route_ids.shape[0]
-    if whole_blocks and lax.axis_size("tp") == 4:
+    fits = lax.axis_size("ep") == 8 and lax.axis_size("tp") == 4
+    if whole_blocks and fits and arrays[0].shape[0] == 4 * WINDOW:
         return shards(*arrays)
     return shards_routed(*arrays)
 

time: 67.9 us -> 61.4 us (0.904)
  Pallas kernels: 63.6 us -> 57.1 us
    pallas_call x1, Pallas kernels: 63.6 us -> 57.1 us  [shards(): pl.pallas_call(functools.partial(layer_kernel, ring), out_shape=(jax.Shap...]
where the time goes in v2:
time: 61.4 us; the launch traced here: 61.2 us
  Pallas kernels  57.1 us (93%)
  local copies, waits for them, and re-layouts  3.44 us (6%)
  between operations  0.65 us (1%)
    pallas_call x1, Pallas kernels, shards(): pl.pallas_call(functools.partial(layer_kernel, ring), out_shape=(jax.Shap...  57.1 us
    unnamed x2, local copies, waits for them, and re-layouts  3.44 us

profile of v2, /device:TPU:0, one launch (start us, length us, event | category | flops | bytes accessed | tf_op | source)
XLA Modules:
  0.0 61.2 jit_solution(5251609529004448138)
XLA Ops:
  0.6 57.1 %layer.1 = (bf16[512,512]{1,0:T(8,128)(2,1)}, bf16[128,512]{1,0:T(8,128)(2,1)}) custom-call(bf16[128,2048]{1,0:T(8,128)(2,1)} %rows_hbm.1, f32[1,2048]{1,0:T(1,128)} %bitcast.13, s32[4,128]{1,0:T(4,128)} %bitcast.15, f32[4,128]{1,0:T(4,128)} %bitcast.16, bf16[512,512]{1,0:T(8,128)(2,1)} %mixer_hbm.1, f32[1,2048]{1,0:T(1,128)} %bitcast.14, f32[1,64]{1,0:T(1,128)} %bitcast.17, ...), custom_call_target="tpu_custom_call" | custom-call | tf_op jit(solution)/shard_map/layer/pallas_call | solution.py:968
  57.8 1.9 %copy.23 = bf16[512,512]{1,0:T(8,128)(2,1)} copy(bf16[512,512]{1,0:T(8,128)(2,1)} %get-tuple-element.4) | data formatting | bytes 1048576
  59.7 1.6 %copy.24 = bf16[128,512]{1,0:T(8,128)(2,1)} copy(bf16[128,512]{1,0:T(8,128)(2,1)} %get-tuple-element.5) | data formatting | bytes 262144

commit v3 on v2

--- a/solution.py
+++ b/solution.py
@@ -275,10 +275,7 @@
     ready,
     going,
     coming,
-    mixer_v,
-    expert_v,
     load_sem,
-    store_sem,
     tok_send,
     ring_recv,
     sib_recv,
@@ -329,7 +326,6 @@
     for device in peers + [sibling, across]:
         pl.semaphore_signal(barrier, inc=1, device_id=device, device_id_type=pl.DeviceIdType.MESH)
 
-    stores = []
 
     def start(copy):
         copy.start()
@@ -668,11 +664,7 @@
             total = total + jnp.dot(
                 att_all[owner, rows, :], out_cols[owner], preferred_element_type=f32
             )
-        mixer_v[rows, :] = total.astype(bf16)
-        stores.append(
-            pltpu.make_async_copy(mixer_v.at[rows, :], mixer_result.at[rows, :], store_sem.at[i])
-        )
-        stores[-1].start()
+        mixer_result[rows, :] = total.astype(bf16)
 
     diagonal = lax.broadcasted_iota(jnp.int32, (block, block), 0) == lax.broadcasted_iota(
         jnp.int32, (block, block), 1
@@ -764,7 +756,7 @@
             total = total + back_wait(direction, 1, b)
             if longest(direction, b) == steps:
                 total = total + back_wait(direction, 2, b)
-        expert_v[rows, :] = total.astype(bf16)
+        expert_result[rows, :] = total.astype(bf16)
 
     with scope("c_h0"):
         loads["gate"].wait()
@@ -901,8 +893,6 @@
     with scope("fin_exp"):
         for b in range(PARTS_BACK):
             finish_expert(b)
-        stores.append(pltpu.make_async_copy(expert_v, expert_result, store_sem.at[pieces]))
-        stores[-1].start()
     with scope("fwd_a0"):
         att.forward(0)
     with scope("out1"):
@@ -910,8 +900,6 @@
     with scope("out0"):
         finish_mixer(0)
     with scope("w_end"):
-        for copy in stores:
-            copy.wait()
         for ref, send in (
             (tok.at[:, pl.ds(0, (ring - 1) * block), :], tok_send.at[0]),
             (mixer_all.at[pl.ds(0, parts - 1)], mix_send.at[0]),
@@ -927,6 +915,17 @@
             (going.at[pl.ds(0, ring - 1)], back_send.at[0]),
         ):
             remote(ref, ref, send, halo_recv.at[0], sibling).wait_send()
+
+
+def settle_kernel(mixer_in, expert_in, mixer_out, expert_out, sem):
+    copies = [
+        pltpu.make_async_copy(mixer_in, mixer_out, sem.at[0]),
+        pltpu.make_async_copy(expert_in, expert_out, sem.at[1]),
+    ]
+    for copy in copies:
+        copy.start()
+    for copy in copies:
+        copy.wait()
 
 
 def shards(
@@ -967,12 +966,9 @@
     dma = pltpu.SemaphoreType.DMA
     outputs = pl.pallas_call(
         functools.partial(layer_kernel, ring),
-        out_shape=(
-            jax.ShapeDtypeStruct((rows_local, out_width), bf16),
-            jax.ShapeDtypeStruct((tokens_local, out_width), bf16),
-        ),
+        out_shape=(vm((rows_local, out_width), bf16), vm((tokens_local, out_width), bf16)),
         in_specs=[hbm] * 19,
-        out_specs=(hbm,) * 2,
+        out_specs=(pl.BlockSpec(memory_space=vm),) * 2,
         scratch_shapes=[
             vm((tokens_local, width), bf16),
             vm((1, width), f32),
@@ -1004,10 +1000,7 @@
             vm((ring * tokens_local, out_width), f32),
             vm((2 * half, tokens_local, out_width), bf16),
             vm((2, half + 1, tokens_local, out_width), bf16),
-            vm((rows_local, out_width), bf16),
-            vm((tokens_local, out_width), bf16),
             dma((17,)),
-            dma((pieces + 1,)),
             dma((1,)),
             dma((2, half, CHUNKS)),
             dma((half,)),
@@ -1055,7 +1048,15 @@
         expert_down[0],
         shared_down,
     )
-    return outputs
+    return pl.pallas_call(
+        settle_kernel,
+        out_shape=tuple(jax.ShapeDtypeStruct(o.shape, o.dtype) for o in outputs),
+        in_specs=[pl.BlockSpec(memory_space=vm)] * 2,
+        out_specs=(hbm,) * 2,
+        scratch_shapes=[dma((2,))],
+        compiler_params=pltpu.CompilerParams(vmem_limit_bytes=1024 * 1024),
+        name="settle",
+    )(*outputs)
 
 
 def plan(*arrays):

time: 61.4 us -> 58.1 us (0.946)
  local copies, waits for them, and re-layouts: 3.44 us -> 0 us
    unnamed x2 -> x0, local copies, waits for them, and re-layouts: 3.44 us -> none
    pallas_call x1 -> x2, Pallas kernels: 57.1 us -> 57.3 us  [the longest x1 56.5 us: shards(): pl.pallas_call(functools.partial(layer_kernel, ring), out_shape=(vm((rows...]
where the time goes in v3:
time: 58.1 us; the launch traced here: 58 us
  Pallas kernels  57.3 us (99%)
  between operations  0.65 us (1%)
    pallas_call x1, Pallas kernels, shards(): pl.pallas_call(functools.partial(layer_kernel, ring), out_shape=(vm((rows...  56.5 us

profile of v3, /device:TPU:0, one launch (start us, length us, event | category | flops | bytes accessed | tf_op | source)
XLA Modules:
  0.0 58.0 jit_solution(10917191322423227738)
XLA Ops:
  0.6 56.5 %layer.1 = (bf16[512,512]{1,0:T(8,128)(2,1)S(1)}, bf16[128,512]{1,0:T(8,128)(2,1)S(1)}) custom-call(bf16[128,2048]{1,0:T(8,128)(2,1)} %rows_hbm.1, f32[1,2048]{1,0:T(1,128)} %bitcast.13, s32[4,128]{1,0:T(4,128)} %bitcast.15, f32[4,128]{1,0:T(4,128)} %bitcast.16, bf16[512,512]{1,0:T(8,128)(2,1)} %mixer_hbm.1, f32[1,2048]{1,0:T(1,128)} %bitcast.14, ...), custom_call_target="tpu_custom_call" | custom-call | tf_op jit(solution)/shard_map/layer/pallas_call | solution.py:967
  57.1 0.8 %settle.1 = (bf16[512,512]{1,0:T(8,128)(2,1)}, bf16[128,512]{1,0:T(8,128)(2,1)}) custom-call(bf16[512,512]{1,0:T(8,128)(2,1)S(1)} %get-tuple-element.4.mixer_in, bf16[128,512]{1,0:T(8,128)(2,1)S(1)} %get-tuple-element.5.expert_in), custom_call_target="tpu_custom_call" | custom-call | tf_op jit(solution)/shard_map/settle/pallas_call | solution.py:1051

commit v4 on v3

--- a/solution.py
+++ b/solution.py
@@ -321,6 +321,7 @@
     shared_width = shared_all.shape[2]
     head_rows = out_cols.shape[1]
     share_rows = head_rows // ring
+    share_piece = share_rows // CHUNKS
 
     barrier = pltpu.get_barrier_semaphore()
     for device in peers + [sibling, across]:
@@ -363,10 +364,11 @@
     load("down", down_hbm, down_v)
     load("shared_down", shared_down_hbm, shared_down_v)
 
+    band_shape = (2 * WINDOW, WINDOW)
     relative = (
-        lax.broadcasted_iota(jnp.int32, (WINDOW, 2 * WINDOW), 0)
+        lax.broadcasted_iota(jnp.int32, band_shape, 1)
         + WINDOW
-        - lax.broadcasted_iota(jnp.int32, (WINDOW, 2 * WINDOW), 1)
+        - lax.broadcasted_iota(jnp.int32, band_shape, 0)
     )
     bias_v[...] = jnp.where((relative >= 0) & (relative < WINDOW), 0.0, -jnp.inf)
     low = lax.broadcasted_iota(jnp.int32, (WINDOW, 2 * HEAD), 1) < HEAD
@@ -499,7 +501,7 @@
 
     tile = 256
 
-    def compute(slots):
+    def compute(slots, now):
         first = min(place_of(slot, ring) for slot in slots) * block
         count = len(slots) * block
 
@@ -513,7 +515,9 @@
 
         lax.fori_loop(0, inner // tile, one, 0)
         for slot in slots:
-            hidden.both(slot)
+            hidden.to_sibling(slot)
+            if slot in now:
+                hidden.to_across(slot)
 
     def project(i):
         rows = pl.ds(i * WINDOW, WINDOW)
@@ -572,31 +576,40 @@
 
     def attend(i):
         rows = pl.ds(i * WINDOW, WINDOW)
+        heads = heads_v.shape[0]
         keys = band_v[pl.ds(i * WINDOW, 2 * WINDOW), pl.ds(0, 2 * HEAD)]
         values = band_v[pl.ds(i * WINDOW, 2 * WINDOW), pl.ds(2 * HEAD, 2 * HEAD)]
         bias = bias_v[...]
         if i == 0:
-            before = lax.broadcasted_iota(jnp.int32, (WINDOW, 2 * WINDOW), 1) < WINDOW
+            before = lax.broadcasted_iota(jnp.int32, band_shape, 0) < WINDOW
             bias = jnp.where(before & (index == 0), -jnp.inf, bias)
-        mixed = []
-        for head in range(heads_v.shape[0]):
-            scores = lax.dot_general(
-                heads_v[head, rows, :],
-                keys,
-                (((1,), (1,)), ((), ())),
-                preferred_element_type=f32,
+        scores = lax.dot_general(
+            keys,
+            heads_v[:, rows, :].reshape(heads * WINDOW, 2 * HEAD),
+            (((1,), (1,)), ((), ())),
+            preferred_element_type=f32,
+        )
+        columns = []
+        for head in range(heads):
+            masked = scores[:, head * WINDOW : (head + 1) * WINDOW] + bias
+            sink = sink_v[:, head : head + 1]
+            peak = jnp.maximum(jnp.max(masked, axis=0, keepdims=True), sink)
+            exponent = jnp.exp(masked - peak)
+            denominator = jnp.sum(exponent, axis=0, keepdims=True) + jnp.exp(sink - peak)
+            columns.append((exponent * (1.0 / denominator)).astype(bf16))
+        mixed = lax.dot_general(
+            values[:, :HEAD],
+            jnp.concatenate(columns, axis=1),
+            (((0,), (0,)), ((), ())),
+            preferred_element_type=f32,
+        )
+        for pair in range(heads // 2):
+            first = 2 * pair * WINDOW
+            two = jnp.concatenate(
+                [mixed[:, first : first + WINDOW], mixed[:, first + WINDOW : first + 2 * WINDOW]],
+                axis=0,
             )
-            masked = scores + bias
-            sink = sink_v[:, head : head + 1]
-            peak = jnp.maximum(jnp.max(masked, axis=1, keepdims=True), sink)
-            exponent = jnp.exp(masked - peak)
-            denominator = jnp.sum(exponent, axis=1, keepdims=True) + jnp.exp(sink - peak)
-            probability = (exponent * (1.0 / denominator)).astype(bf16)
-            mixed.append(jnp.dot(probability, values, preferred_element_type=f32))
-        for pair in range(len(mixed) // 2):
-            att_all[part, rows, pl.ds(pair * 2 * HEAD, 2 * HEAD)] = jnp.where(
-                low, mixed[2 * pair], mixed[2 * pair + 1]
-            ).astype(bf16)
+            att_all[part, rows, pl.ds(pair * 2 * HEAD, 2 * HEAD)] = two.T.astype(bf16)
 
     chip_cols = 2 * out_width
 
@@ -623,15 +636,31 @@
             )
         )
 
+    def stage_ref(slot, chunk):
+        owner = peer_index[(ring - slot) % ring]
+        first = owner * share_rows + chunk * share_piece
+        return out_stage.at[pl.ds(pl.multiple_of(first, share_piece), share_piece), :]
+
+    def column_hop(direction, distance, chunk):
+        here = stage_ref(slot_at(direction, distance - 1, ring) % ring, chunk)
+        to = ahead if direction == 0 else behind
+        start(remote(here, here, wring_send.at[0], wring_recv.at[distance - 1], to))
+
     def column_start():
         mine = out_stage.at[pl.ds(pl.multiple_of(index * share_rows, share_rows), share_rows), :]
         remote(mine, mine, wcol_send.at[1], wcol_recv.at[1], across).wait_recv()
-        for device in peers:
-            start(remote(mine, mine, wring_send.at[0], wring_recv.at[0], device))
-
-    def column_rest():
-        here = out_stage.at[pl.ds(0, (ring - 1) * share_rows), :]
-        remote(here, here, wring_send.at[0], wring_recv.at[0], sibling).wait_recv()
+        for chunk in range(CHUNKS):
+            for direction in range(2):
+                column_hop(direction, 1, chunk)
+
+    def column_arrive(distance):
+        count = 2 if distance < steps else 1
+        here = out_stage.at[pl.ds(0, count * share_rows), :]
+        remote(here, here, wring_send.at[0], wring_recv.at[distance - 1], sibling).wait_recv()
+        for chunk in range(CHUNKS):
+            for direction in range(2):
+                if distance < limit(direction, chunk, ring):
+                    column_hop(direction, distance + 1, chunk)
 
     def column_swap():
         start(
@@ -761,9 +790,10 @@
     with scope("c_h0"):
         loads["gate"].wait()
         loads["up"].wait()
-        compute([0])
+        compute([0], [])
     spread_columns()
     mixer.to_across(1)
+    mixer.to_across(0)
     with scope("A1c0"):
         arrive(1, 0)
     with scope("fwd_m3"):
@@ -781,7 +811,7 @@
     with scope("S1"):
         swapped(1)
     with scope("c_h1"):
-        compute([1, ring - 1])
+        compute([1, ring - 1], [1, ring - 1])
     with scope("A2c0"):
         arrive(2, 0)
     with scope("qkv2"):
@@ -789,100 +819,118 @@
     with scope("att3"):
         attend(3)
         att.to_sibling(3)
+    with scope("fwd_sh_m1"):
+        shared.forward(0)
+        mixer.forward(1)
     with scope("A2c1"):
         arrive(2, 1)
-    with scope("fwd_sh_h0"):
-        shared.forward(0)
-        hidden.forward(0)
     with scope("S2"):
         swapped(2)
     with scope("c_h2"):
-        compute([2, ring - 2])
+        compute([2, ring - 2], [2])
     with scope("A3c0"):
         arrive(3, 0)
-    with scope("fwd_m1"):
-        mixer.forward(1)
-    with scope("own"):
-        loads["down"].wait()
-        loads["shared_down"].wait()
-        here = dense_all.at[pl.ds(1, ring - 1)]
-        remote(here, here, dense_send.at[0], dense_recv.at[0], sibling).wait_recv()
-        own_rows()
+    with scope("fwd_m0"):
+        mixer.forward(0)
+    att.to_across(3)
     with scope("qkv1"):
         project(1)
+    with scope("att2"):
+        attend(2)
+        att.to_sibling(2)
     with scope("A3c1"):
         arrive(3, 1)
     with scope("w0"):
         column_start()
     with scope("fwd_h1"):
         hidden.forward(1)
+    with scope("qkv0"):
+        project(0)
     with scope("S3"):
         swapped(3)
     with scope("c_h3"):
-        compute([3, ring - 3])
+        compute([3, ring - 3], [3, ring - 3])
     with scope("A4"):
         arrive(4, 0)
+    with scope("w1"):
+        column_arrive(1)
     with scope("fwd_h7"):
         hidden.forward(ring - 1)
-    with scope("att2"):
-        attend(2)
-        att.to_sibling(2)
+    with scope("att1"):
+        attend(1)
+        att.to_sibling(1)
+    with scope("halo"):
+        wait_halo()
+    with scope("att0"):
+        attend(0)
+        att.to_sibling(0)
     with scope("S4"):
         swapped(4)
     with scope("c_h4"):
-        compute([4])
-    mixer.to_across(0)
-    att.to_across(3)
-    att.to_across(2)
+        compute([4], [4])
+    hidden.to_across(ring - 2)
+    hidden.to_across(0)
+    for i in (2, 1, 0):
+        att.to_across(i)
+    with scope("fwd_h2"):
+        hidden.forward(2)
+    with scope("w_dense"):
+        loads["down"].wait()
+        loads["shared_down"].wait()
+        here = dense_all.at[pl.ds(1, ring - 1)]
+        remote(here, here, dense_send.at[0], dense_recv.at[0], sibling).wait_recv()
     with scope("down1"):
         weighted([1, ring - 1])
-    push(1, True)
-    with scope("fwd_h2"):
-        hidden.forward(2)
-        hidden.forward(ring - 2)
-    with scope("halo"):
-        wait_halo()
+        push(1, True)
+    with scope("w2"):
+        column_arrive(2)
+    with scope("down2"):
+        weighted([2])
     with scope("fwd_h3"):
+        att.forward(3)
         hidden.forward(3)
-    with scope("down2"):
-        weighted([2, ring - 2])
     with scope("down3"):
         weighted([3])
         push(3, False, (1,))
         push(3, True, (1,))
     with scope("fwd_h5"):
         hidden.forward(ring - 3)
-    with scope("col_rest"):
-        column_rest()
-        column_swap()
+    with scope("w3"):
+        column_arrive(3)
     with scope("down5"):
         weighted([ring - 3])
         push(3, False, (0,))
         push(3, True, (0,))
     with scope("fwd_h4"):
         hidden.forward(4)
+    with scope("push2s1"):
+        push(2, False, (1,))
     with scope("down4"):
         weighted([4])
         push(4, True)
-    with scope("fwd_m0"):
-        mixer.forward(0)
-    with scope("push2s"):
-        push(2, False)
-    with scope("qkv0"):
-        project(0)
-    with scope("att1"):
-        attend(1)
-        att.both(1)
-    with scope("push2l"):
-        push(2, True)
-    with scope("push1s"):
-        push(1, False)
-    with scope("att0"):
-        attend(0)
-        att.both(0)
-    with scope("fwd_a32"):
-        att.forward(3)
+    with scope("fwd_h6"):
+        hidden.forward(ring - 2)
+    with scope("w4"):
+        column_arrive(4)
+        column_swap()
+    with scope("down6"):
+        weighted([ring - 2])
+    with scope("push1s1"):
+        push(1, False, (1,))
+    with scope("push2s0"):
+        push(2, False, (0,))
+    with scope("fwd_h0"):
+        hidden.forward(0)
+    with scope("push2l1"):
+        push(2, True, (1,))
+    with scope("push2l0"):
+        push(2, True, (0,))
+    with scope("fwd_a2"):
         att.forward(2)
+    with scope("own"):
+        own_rows()
+    with scope("push1s0"):
+        push(1, False, (0,))
     with scope("fwd_a1"):
         att.forward(1)
     with scope("out3"):
@@ -890,15 +938,15 @@
         finish_mixer(3)
     with scope("out2"):
         finish_mixer(2)
-    with scope("fin_exp"):
-        for b in range(PARTS_BACK):
-            finish_expert(b)
     with scope("fwd_a0"):
         att.forward(0)
     with scope("out1"):
         finish_mixer(1)
     with scope("out0"):
         finish_mixer(0)
+    with scope("fin_exp"):
+        for b in range(PARTS_BACK):
+            finish_expert(b)
     with scope("w_end"):
         for ref, send in (
             (tok.at[:, pl.ds(0, (ring - 1) * block), :], tok_send.at[0]),
@@ -996,7 +1044,7 @@
             vm((WINDOW, parts * mixer_cols), bf16),
             vm((head_width // HEAD, rows_local, 2 * HEAD), bf16),
             vm((WINDOW + rows_local, 4 * HEAD), bf16),
-            vm((WINDOW, 2 * WINDOW), f32),
+            vm((2 * WINDOW, WINDOW), f32),
             vm((ring * tokens_local, out_width), f32),
             vm((2 * half, tokens_local, out_width), bf16),
             vm((2, half + 1, tokens_local, out_width), bf16),
@@ -1019,7 +1067,7 @@
             dma((3,)),
             dma((3,)),
             dma((1,)),
-            dma((1,)),
+            dma((half,)),
             dma((1,)),
             dma((2, half, PARTS_BACK)),
         ],

time: 58.1 us -> 55.2 us (0.950)
  Pallas kernels: 57.3 us -> 54.4 us
    pallas_call x1, Pallas kernels: 56.5 us -> 53.5 us  [shards(): pl.pallas_call(functools.partial(layer_kernel, ring), out_shape=(vm((rows...]
where the time goes in v4:
time: 55.2 us; the launch traced here: 55 us
  Pallas kernels  54.4 us (99%)
  between operations  0.65 us (1%)
    pallas_call x1, Pallas kernels, shards(): pl.pallas_call(functools.partial(layer_kernel, ring), out_shape=(vm((rows...  53.5 us

profile of v4, /device:TPU:0, one launch (start us, length us, event | category | flops | bytes accessed | tf_op | source)
XLA Modules:
  0.0 55.0 jit_solution(17833021542413128744)
XLA Ops:
  0.6 53.5 %layer.1 = (bf16[512,512]{1,0:T(8,128)(2,1)S(1)}, bf16[128,512]{1,0:T(8,128)(2,1)S(1)}) custom-call(bf16[128,2048]{1,0:T(8,128)(2,1)} %rows_hbm.1, f32[1,2048]{1,0:T(1,128)} %bitcast.13, s32[4,128]{1,0:T(4,128)} %bitcast.15, f32[4,128]{1,0:T(4,128)} %bitcast.16, bf16[512,512]{1,0:T(8,128)(2,1)} %mixer_hbm.1, f32[1,2048]{1,0:T(1,128)} %bitcast.14, ...), custom_call_target="tpu_custom_call" | custom-call | tf_op jit(solution)/shard_map/layer/pallas_call | solution.py:1015
  54.2 0.8 %settle.1 = (bf16[512,512]{1,0:T(8,128)(2,1)}, bf16[128,512]{1,0:T(8,128)(2,1)}) custom-call(bf16[512,512]{1,0:T(8,128)(2,1)S(1)} %get-tuple-element.4.mixer_in, bf16[128,512]{1,0:T(8,128)(2,1)S(1)} %get-tuple-element.5.expert_in), custom_call_target="tpu_custom_call" | custom-call | tf_op jit(solution)/shard_map/settle/pallas_call | solution.py:1099

commit v5 on v4

--- a/solution.py
+++ b/solution.py
@@ -832,7 +832,6 @@
         arrive(3, 0)
     with scope("fwd_m0"):
         mixer.forward(0)
-    att.to_across(3)
     with scope("qkv1"):
         project(1)
     with scope("att2"):
@@ -849,7 +848,8 @@
     with scope("S3"):
         swapped(3)
     with scope("c_h3"):
-        compute([3, ring - 3], [3, ring - 3])
+        compute([3], [3])
+        compute([ring - 3], [ring - 3])
     with scope("A4"):
         arrive(4, 0)
     with scope("w1"):
@@ -870,7 +870,7 @@
         compute([4], [4])
     hidden.to_across(ring - 2)
     hidden.to_across(0)
-    for i in (2, 1, 0):
+    for i in (3, 2, 1, 0):
         att.to_across(i)
     with scope("fwd_h2"):
         hidden.forward(2)
@@ -887,7 +887,6 @@
     with scope("down2"):
         weighted([2])
     with scope("fwd_h3"):
-        att.forward(3)
         hidden.forward(3)
     with scope("down3"):
         weighted([3])
@@ -925,12 +924,13 @@
         push(2, True, (1,))
     with scope("push2l0"):
         push(2, True, (0,))
+    with scope("push1s0"):
+        push(1, False, (0,))
     with scope("fwd_a2"):
+        att.forward(3)
         att.forward(2)
     with scope("own"):
         own_rows()
-    with scope("push1s0"):
-        push(1, False, (0,))
     with scope("fwd_a1"):
         att.forward(1)
     with scope("out3"):

time: 55.2 us -> 54.8 us (level)
  no operation moved by 1% of the time
where the time goes in v5:
time: 54.8 us; the launch traced here: 54.6 us
  Pallas kernels  54 us (99%)
  between operations  0.65 us (1%)
    pallas_call x1, Pallas kernels, shards(): pl.pallas_call(functools.partial(layer_kernel, ring), out_shape=(vm((rows...  53.1 us

profile of v5, /device:TPU:0, one launch (start us, length us, event | category | flops | bytes accessed | tf_op | source)
XLA Modules:
  0.0 54.6 jit_solution(17667431911760659312)
XLA Ops:
  0.6 53.1 %layer.1 = (bf16[512,512]{1,0:T(8,128)(2,1)S(1)}, bf16[128,512]{1,0:T(8,128)(2,1)S(1)}) custom-call(bf16[128,2048]{1,0:T(8,128)(2,1)} %rows_hbm.1, f32[1,2048]{1,0:T(1,128)} %bitcast.13, s32[4,128]{1,0:T(4,128)} %bitcast.15, f32[4,128]{1,0:T(4,128)} %bitcast.16, bf16[512,512]{1,0:T(8,128)(2,1)} %mixer_hbm.1, f32[1,2048]{1,0:T(1,128)} %bitcast.14, ...), custom_call_target="tpu_custom_call" | custom-call | tf_op jit(solution)/shard_map/layer/pallas_call | solution.py:1015
  53.8 0.8 %settle.1 = (bf16[512,512]{1,0:T(8,128)(2,1)}, bf16[128,512]{1,0:T(8,128)(2,1)}) custom-call(bf16[512,512]{1,0:T(8,128)(2,1)S(1)} %get-tuple-element.4.mixer_in, bf16[128,512]{1,0:T(8,128)(2,1)S(1)} %get-tuple-element.5.expert_in), custom_call_target="tpu_custom_call" | custom-call | tf_op jit(solution)/shard_map/settle/pallas_call | solution.py:1099

commit v6 on v5

--- a/solution.py
+++ b/solution.py
@@ -683,13 +683,16 @@
 
     def finish_mixer(i):
         rows = pl.ds(i * WINDOW, WINDOW)
-        att.rest(i)
         total = jnp.dot(
             att_all[across_part, rows, :],
             out_stage[:, pl.ds(pl.multiple_of(core * out_width, out_width), out_width)],
             preferred_element_type=f32,
         )
-        for owner in (part, sib_part, corner_part):
+        total = total + jnp.dot(
+            att_all[part, rows, :], out_cols[part], preferred_element_type=f32
+        )
+        att.rest(i)
+        for owner in (sib_part, corner_part):
             total = total + jnp.dot(
                 att_all[owner, rows, :], out_cols[owner], preferred_element_type=f32
             )
@@ -704,21 +707,20 @@
         return jnp.sum(jnp.where(diagonal, row, 0.0), axis=1, keepdims=True)
 
     def weighted(slots):
+        first = min(place_of(slot, ring) for slot in slots) * block
+        count = len(slots) * block
+
+        def share(owner):
+            return jnp.dot(
+                hidden_all[owner, pl.ds(first, count), :],
+                down_v[pl.ds(pl.multiple_of(owner * inner, inner), inner), :],
+                preferred_element_type=f32,
+            )
+
+        total = share(part) + share(across_part)
         for slot in slots:
             hidden.rest(slot)
-        first = min(place_of(slot, ring) for slot in slots) * block
-        count = len(slots) * block
-        total = jnp.dot(
-            hidden_all[0, pl.ds(first, count), :],
-            down_v[pl.ds(0, inner), :],
-            preferred_element_type=f32,
-        )
-        for owner in range(1, parts):
-            total = total + jnp.dot(
-                hidden_all[owner, pl.ds(first, count), :],
-                down_v[pl.ds(owner * inner, inner), :],
-                preferred_element_type=f32,
-            )
+        total = total + share(sib_part) + share(corner_part)
         rounded = total.astype(bf16).astype(f32)
         ordered = sorted(slots, key=lambda slot: place_of(slot, ring))
         ready[pl.ds(first, count), :] = rounded * jnp.concatenate(

time: 54.8 us -> 54.7 us (level)
  no operation moved by 1% of the time
where the time goes in v6:
time: 54.7 us; the launch traced here: 54.5 us
  Pallas kernels  53.9 us (99%)
  between operations  0.65 us (1%)
    pallas_call x1, Pallas kernels, shards(): pl.pallas_call(functools.partial(layer_kernel, ring), out_shape=(vm((rows...  53.1 us

profile of v6, /device:TPU:0, one launch (start us, length us, event | category | flops | bytes accessed | tf_op | source)
XLA Modules:
  0.0 54.5 jit_solution(7694021001785862630)
XLA Ops:
  0.6 53.1 %layer.1 = (bf16[512,512]{1,0:T(8,128)(2,1)S(1)}, bf16[128,512]{1,0:T(8,128)(2,1)S(1)}) custom-call(bf16[128,2048]{1,0:T(8,128)(2,1)} %rows_hbm.1, f32[1,2048]{1,0:T(1,128)} %bitcast.13, s32[4,128]{1,0:T(4,128)} %bitcast.15, f32[4,128]{1,0:T(4,128)} %bitcast.16, bf16[512,512]{1,0:T(8,128)(2,1)} %mixer_hbm.1, f32[1,2048]{1,0:T(1,128)} %bitcast.14, ...), custom_call_target="tpu_custom_call" | custom-call | tf_op jit(solution)/shard_map/layer/pallas_call | solution.py:1017
  53.7 0.8 %settle.1 = (bf16[512,512]{1,0:T(8,128)(2,1)}, bf16[128,512]{1,0:T(8,128)(2,1)}) custom-call(bf16[512,512]{1,0:T(8,128)(2,1)S(1)} %get-tuple-element.4.mixer_in, bf16[128,512]{1,0:T(8,128)(2,1)S(1)} %get-tuple-element.5.expert_in), custom_call_target="tpu_custom_call" | custom-call | tf_op jit(solution)/shard_map/settle/pallas_call | solution.py:1101
